TPU v7x, 512 devices: a whole 4x8x8 slice. The times are simulated.
512 devices in a mesh: sp: 32 (over z, x), tp: 16 (over y, core).
Axes of the slice: x: 4, y: 8, z: 8, core: 2. Of those that a mesh axis runs over, the one named last changes fastest.
Arguments:
- residual_layer_input: bfloat16 [8192, 2048], P(('sp', 'tp')), may hold values from -6 to 6
- value_projected: bfloat16 [8192, 4096], P('sp', 'tp'), may hold values from -6 to 6
- key_projected: bfloat16 [8192, 2048], P('sp', 'tp'), may hold values from -6 to 6
- query_projected: bfloat16 [8192, 2048], P('sp', 'tp'), may hold values from -6 to 6
- output_gate_projected: bfloat16 [8192, 4096], P('sp', 'tp'), may hold values from -6 to 6
- step_projected_raw: bfloat16 [2, 8192, 64], P(None, 'sp', 'tp'), may hold values from -5.5 to 5
- head_decay_logarithm: float32 [2, 64], P(None, 'tp'), may hold values from -15 to -2.9
- position_extra_decay: float32 [8192, 64], P('sp', 'tp'), may hold values from -2.1 to 0
- value_filter_weight: bfloat16 [5, 4096], P(None, 'tp'), may hold values from -2.5 to 2.5
- key_filter_weight: bfloat16 [5, 2048], P(None, 'tp'), may hold values from -2.5 to 2.5
- query_filter_weight: bfloat16 [5, 2048], P(None, 'tp'), may hold values from -2.5 to 2.5
- head_norm_gain: float32 [4096], P('tp'), may hold values from 0.1 to 1.9
- mixer_output_matrix: bfloat16 [4096, 2048], P(None, 'tp'), may hold values from -0.09375 to 0.09375
- expert_norm_gain: float32 [2048], replicated, may hold values from 0.1 to 1.9
- routes: int32 [8192, 2], P('sp'), may hold values from 0 to 31, all different within a row; in each aligned block of 16 rows (0 to 15, 16 to 31, ...) at most 2 rows name the same one
- chosen_expert_weight: float32 [8192, 2], P(('sp', 'tp')), may hold values from 0.1 to 1
- expert_gate_matrix: bfloat16 [32, 2048, 4096], P('sp', None, 'tp'), may hold values from -0.125 to 0.125
- expert_up_matrix: bfloat16 [32, 2048, 4096], P('sp', None, 'tp'), may hold values from -0.125 to 0.125
- expert_down_matrix: bfloat16 [32, 4096, 2048], P('sp', 'tp'), may hold values from -0.09375 to 0.09375
Outputs:
- layer_output: bfloat16 [8192, 2048], P(('sp', 'tp'))
Inputs may be any that keep to these rules, and one draw needn't show every extreme that they name: `routes`: each row names 2 different experts; the rows of one device (aligned blocks of 16 rows) name one expert 2 times at most, and that most is reached.
All inputs are finite; a program needn't handle non-finite values.
Results may differ from a plain program's by a relative error of at most 0.015.
Values may be sent and summed in bfloat16 or wider, within the bound.
A program may use at most 64 MiB of HBM per device.

v0:
```python
import jax
import jax.numpy as jnp
from jax import lax
from jax.sharding import Mesh
from jax.sharding import PartitionSpec as P

HEAD_DIM = 64
STATE = 128
BLOCK = 128
TAPS = 5
SP = ("sp_0", "sp_1")
TP = ("tp_0", "tp_1")
SP_TP = ("sp_0", "sp_1", "tp_0", "tp_1")


epsilon = 1e-06


def padded_2(cells, sides, width):
    for axis, dim in sides:
        count = lax.axis_size(axis)
        ends = count - 1
        head = lax.slice_in_dim(cells, 0, width, axis=dim)
        tail = lax.slice_in_dim(cells, cells.shape[dim] - width, cells.shape[dim], axis=dim)
        cells = jnp.concatenate(
            [
                lax.ppermute(tail, axis, [(i, (i + 1) % count) for i in range(ends)]),
                cells,
                lax.ppermute(head, axis, [((i + 1) % count, i) for i in range(ends)]),
            ],
            axis=dim,
        )
    return cells


def filled_with(x, identity):
    return jax.tree.map(
        lambda part, zero: jnp.zeros_like(part) + jnp.asarray(zero, part.dtype), x, identity
    )


def carried_in(x, axes, combine, identity, reverse):
    before = start = filled_with(x, identity)
    so_far = x
    for axis in reversed(axes):
        count, here = (lax.axis_size(axis), lax.axis_index(axis))
        pieces = jax.tree.map(
            lambda part, kind: lax.all_gather(part.astype(kind), axis),
            so_far,
            (jnp.bfloat16, jnp.bfloat16),
        )
        inside, so_far = (start, start)
        for k in reversed(range(count)) if reverse else range(count):
            passed = k > here if reverse else k < here
            so_far = combine(
                so_far, jax.tree.map(lambda part, own: part[k].astype(own.dtype), pieces, x)
            )
            inside = jax.tree.map(lambda new, old: jnp.where(passed, new, old), so_far, inside)
        before = combine(inside, before)
    return before


def gather_axes(x, axes, dim):
    filled = x
    for number in range(len(axes) - 1, -1, -1):
        filled = lax.all_gather(filled, axes[number], axis=dim, tiled=True)
    return filled


def prefix_matrix(length):
    row_index = lax.broadcasted_iota(jnp.int32, (length, length), 0)
    column_index = lax.broadcasted_iota(jnp.int32, (length, length), 1)
    return (column_index <= row_index).astype(jnp.float32)


def carry_combine(first_part, second_part):
    return (
        first_part[0] + second_part[0],
        jnp.exp(second_part[0])[..., None, None] * first_part[1] + second_part[1],
    )


def local_chain(states, totals, reverse):

    def advance(carried, operands):
        block_state, block_total = operands
        return (jnp.exp(block_total)[..., None, None] * carried + block_state, carried)

    start_state = jnp.zeros(states.shape[1:], jnp.float32)
    return lax.scan(advance, start_state, (states, totals), reverse=reverse)


def mix_tokens(
    value_projected,
    key_projected,
    query_projected,
    output_gate_projected,
    step_projected_raw,
    head_decay_logarithm,
    position_extra_decay,
    value_filter_weight,
    key_filter_weight,
    query_filter_weight,
    head_norm_gain,
):
    tokens = value_projected.shape[0]
    value_width = value_projected.shape[1]
    key_width = key_projected.shape[1]
    head_count = step_projected_raw.shape[2]
    group_count = key_width // STATE
    per_group = head_count // group_count
    blocks = tokens // BLOCK
    joined = jnp.concatenate([value_projected, key_projected, query_projected], axis=1)
    padded = padded_2(joined, ((SP, 0),), (TAPS - 1) // 2).astype(jnp.float32)
    weights = jnp.concatenate(
        [value_filter_weight, key_filter_weight, query_filter_weight], axis=1
    ).astype(jnp.float32)
    filtered = weights[0] * padded[0:tokens]
    for offset in range(1, TAPS):
        filtered = filtered + weights[offset] * padded[offset : offset + tokens]
    values = filtered[:, :value_width].astype(jnp.bfloat16)
    key_rows = jax.nn.silu(filtered[:, value_width : value_width + key_width]).astype(jnp.bfloat16)
    key_rows = key_rows.reshape(blocks, BLOCK, group_count, STATE)
    query_rows = jax.nn.silu(filtered[:, value_width + key_width :]).astype(jnp.bfloat16)
    query_rows = query_rows.reshape(blocks, BLOCK, group_count, STATE)
    positive_step_sizes = jax.nn.softplus(step_projected_raw.astype(jnp.float32))
    decay_logarithm = (
        -jnp.exp(head_decay_logarithm)[:, None, :] * positive_step_sizes
        + position_extra_decay[None]
    )
    scaled = (
        values.astype(jnp.float32).reshape(tokens, head_count, HEAD_DIM)[None]
        * positive_step_sizes[..., None]
    ).astype(jnp.bfloat16)
    scaled = scaled.reshape(2, blocks, BLOCK, group_count, per_group, HEAD_DIM)
    log_blocks = decay_logarithm.reshape(2, blocks, BLOCK, group_count, per_group)
    running = jnp.einsum("ls,dbsgh->dblgh", prefix_matrix(BLOCK), log_blocks)
    forward_cum = running[0]
    backward_excl = running[1] - log_blocks[1]
    forward_total = running[0][:, -1]
    backward_total = running[1][:, -1]
    scores = jnp.einsum("blgn,bsgn->blsg", query_rows, key_rows, preferred_element_type=jnp.float32)
    position = lax.broadcasted_iota(jnp.int32, (BLOCK,), 0)
    lower_mask = (position[None, :] <= position[:, None])[None, :, :, None, None]
    upper_mask = (position[None, :] >= position[:, None])[None, :, :, None, None]
    forward_gap = jnp.where(lower_mask, forward_cum[:, :, None] - forward_cum[:, None, :], -jnp.inf)
    backward_gap = jnp.where(
        upper_mask, backward_excl[:, None, :] - backward_excl[:, :, None], -jnp.inf
    )
    forward_weight = (scores[..., None] * jnp.exp(forward_gap)).astype(jnp.bfloat16)
    backward_weight = (scores[..., None] * jnp.exp(backward_gap)).astype(jnp.bfloat16)
    inner = jnp.einsum(
        "blsgh,bsghp->blghp", forward_weight, scaled[0], preferred_element_type=jnp.float32
    )
    inner = inner + jnp.einsum(
        "blsgh,bsghp->blghp", backward_weight, scaled[1], preferred_element_type=jnp.float32
    )
    key_wide = key_rows.astype(jnp.float32)[:, :, :, None, :]
    forward_keys = (jnp.exp(forward_total[:, None] - forward_cum)[..., None] * key_wide).astype(
        jnp.bfloat16
    )
    backward_keys = (jnp.exp(backward_excl)[..., None] * key_wide).astype(jnp.bfloat16)
    forward_state = jnp.einsum(
        "bsghn,bsghp->bghpn", forward_keys, scaled[0], preferred_element_type=jnp.float32
    )
    backward_state = jnp.einsum(
        "bsghn,bsghp->bghpn", backward_keys, scaled[1], preferred_element_type=jnp.float32
    )
    forward_final, forward_before = local_chain(forward_state, forward_total, False)
    backward_final, backward_before = local_chain(backward_state, backward_total, True)
    forward_sum = jnp.sum(forward_total, axis=0)
    backward_sum = jnp.sum(backward_total, axis=0)
    zero_total = jnp.zeros(forward_sum.shape, jnp.float32)
    zero_state = jnp.zeros(forward_final.shape, jnp.float32)
    entering = carried_in(
        (forward_sum, forward_final), SP, carry_combine, (zero_total, zero_state), False
    )[1]
    leaving = carried_in(
        (backward_sum, backward_final), SP, carry_combine, (zero_total, zero_state), True
    )[1]
    forward_prior = jnp.cumsum(forward_total, axis=0) - forward_total
    backward_after = backward_sum[None] - jnp.cumsum(backward_total, axis=0)
    forward_in = jnp.exp(forward_prior)[..., None, None] * entering[None] + forward_before
    backward_in = jnp.exp(backward_after)[..., None, None] * leaving[None] + backward_before
    forward_read = jnp.exp(forward_cum)[..., None] * jnp.einsum(
        "blgn,bghpn->blghp",
        query_rows,
        forward_in.astype(jnp.bfloat16),
        preferred_element_type=jnp.float32,
    )
    backward_read = jnp.exp(backward_total[:, None] - backward_excl)[..., None] * jnp.einsum(
        "blgn,bghpn->blghp",
        query_rows,
        backward_in.astype(jnp.bfloat16),
        preferred_element_type=jnp.float32,
    )
    mixer_raw = (inner + forward_read + backward_read).reshape(tokens, head_count, HEAD_DIM)
    gated = mixer_raw * jax.nn.silu(output_gate_projected.astype(jnp.float32)).reshape(
        tokens, head_count, HEAD_DIM
    )
    inverse_rms = lax.rsqrt(jnp.mean(gated * gated, axis=-1, keepdims=True) + epsilon)
    head_normed = (gated * inverse_rms * head_norm_gain.reshape(head_count, HEAD_DIM)).astype(
        jnp.bfloat16
    )
    return head_normed.reshape(tokens, head_count * HEAD_DIM)


def slot_table(route_rows, experts, capacity):
    flat_ids = route_rows.reshape(-1)
    expert_ids = lax.broadcasted_iota(jnp.int32, (flat_ids.shape[0], experts), 1)
    matches = (flat_ids[:, None] == expert_ids).astype(jnp.int32)
    earlier = jnp.cumsum(matches, axis=0) - matches
    rank_in = jnp.sum(matches * earlier, axis=1)
    return (flat_ids * capacity + rank_in).reshape(route_rows.shape)


def dispatch_rows(slots, token_rows, places):
    place_ids = lax.broadcasted_iota(jnp.int32, (places,) + slots.shape, 0)
    one_hot = jnp.sum((place_ids == slots[None]).astype(jnp.float32), axis=2).astype(jnp.bfloat16)
    return jnp.dot(one_hot, token_rows, preferred_element_type=jnp.float32).astype(jnp.bfloat16)


def shards(
    residual_layer_input,
    value_projected,
    key_projected,
    query_projected,
    output_gate_projected,
    step_projected_raw,
    head_decay_logarithm,
    position_extra_decay,
    value_filter_weight,
    key_filter_weight,
    query_filter_weight,
    head_norm_gain,
    mixer_output_matrix,
    expert_norm_gain,
    routes,
    chosen_expert_weight,
    expert_gate_matrix,
    expert_up_matrix,
    expert_down_matrix,
):
    heads_out = mix_tokens(
        value_projected,
        key_projected,
        query_projected,
        output_gate_projected,
        step_projected_raw,
        head_decay_logarithm,
        position_extra_decay,
        value_filter_weight,
        key_filter_weight,
        query_filter_weight,
        head_norm_gain,
    )
    projected = jnp.dot(
        gather_axes(heads_out, TP, 1), mixer_output_matrix, preferred_element_type=jnp.float32
    ).astype(jnp.bfloat16)
    mixer_out = lax.all_to_all(projected, TP, split_axis=0, concat_axis=1, tiled=True)
    middle = (residual_layer_input.astype(jnp.float32) + mixer_out.astype(jnp.float32)).astype(
        jnp.bfloat16
    )
    residual = middle.astype(jnp.float32)
    normed = (
        residual
        * lax.rsqrt(jnp.mean(residual * residual, axis=-1, keepdims=True) + epsilon)
        * expert_norm_gain
    ).astype(jnp.bfloat16)
    own_rows = normed.shape[0]
    model_width = normed.shape[1]
    top_count = routes.shape[1]
    experts = lax.axis_size(SP)
    capacity = 2 * own_rows * top_count // experts
    places = experts * capacity
    position = lax.axis_index(TP)
    own_routes = lax.dynamic_slice_in_dim(routes, position * own_rows, own_rows, 0)
    own_slots = slot_table(own_routes, experts, capacity)
    outgoing = dispatch_rows(own_slots, normed, places)
    received = lax.all_to_all(
        outgoing.reshape(experts, capacity, model_width),
        SP,
        split_axis=0,
        concat_axis=0,
        tiled=True,
    )
    arrived = lax.all_gather(received[None], TP, axis=0, tiled=True)
    slot_rows = arrived.reshape(-1, model_width)
    gate_value = jnp.dot(slot_rows, expert_gate_matrix[0], preferred_element_type=jnp.float32)
    up_value = jnp.dot(slot_rows, expert_up_matrix[0], preferred_element_type=jnp.float32)
    hidden = (jax.nn.silu(gate_value) * up_value).astype(jnp.bfloat16)
    partial_sum = jnp.dot(hidden, expert_down_matrix[0], preferred_element_type=jnp.float32).astype(
        jnp.bfloat16
    )
    summed = lax.psum_scatter(
        partial_sum.astype(jnp.float32).reshape(arrived.shape).astype(jnp.bfloat16),
        TP,
        scatter_dimension=0,
        tiled=True,
    )
    results = summed.reshape(experts, capacity, model_width)
    returned = lax.all_to_all(results, SP, split_axis=0, concat_axis=0, tiled=True)
    chosen = (
        lax.broadcasted_iota(jnp.int32, (own_rows, top_count, places), 2) == own_slots[:, :, None]
    )
    mixing = jnp.sum(jnp.where(chosen, chosen_expert_weight[:, :, None], 0.0), axis=1)
    expert_mix = jnp.dot(mixing, returned.reshape(places, model_width).astype(jnp.float32))
    return (residual + expert_mix).astype(jnp.bfloat16)


def solution(mesh):
    finer = Mesh(mesh.devices.reshape(8, 4, 8, 2), ("sp_0", "sp_1", "tp_0", "tp_1"))
    return jax.shard_map(
        shards,
        mesh=finer,
        in_specs=(
            P(SP_TP, None),
            P(SP, TP),
            P(SP, TP),
            P(SP, TP),
            P(SP, TP),
            P(None, SP, TP),
            P(None, TP),
            P(SP, TP),
            P(None, TP),
            P(None, TP),
            P(None, TP),
            P(TP),
            P(None, TP),
            P(),
            P(SP, None),
            P(SP_TP, None),
            P(SP, None, TP),
            P(SP, None, TP),
            P(SP, TP, None),
        ),
        out_specs=P(SP_TP, None),
        check_vma=False,
    )
```

profile of v0, /device:TPU:6, one launch (start us, length us, event | category | flops | bytes accessed | tf_op | source)
XLA Modules:
  0.0 410.5 jit_solution(13802664168214537956)
XLA Ops:
  9.7 4.2 %collective-permute-start = (bf16[2,512]{0,1:T(8,128)(2,1)S(1)}, bf16[2,512]{0,1:T(8,128)(2,1)S(1)}, u32[]{:S(2)}, u32[]{:S(2)}) collective-permute-start(bf16[2,512]{0,1:T(8,128)(2,1)S(1)} %get-tuple-element.275), channel_id=1, source_target_pairs={{0,16},{16,32},{32,48},{48,64},{64,80},{80,96},{96,112},{112,128},... | collective-permute-start | bytes 6152 | tf_op jit(solution)/shard_map/ppermute | solution.py:27
  13.9 1.9 collective-permute-start.1
  21.9 9.2 %all-reduce.2 = (bf16[16]{0:T(256)(128)(2,1)S(1)}, bf16[16]{0:T(256)(128)(2,1)S(1)}) all-reduce(bf16[16]{0:T(256)(128)(2,1)S(1)} %dynamic-update-slice.1, bf16[16]{0:T(256)(128)(2,1)S(1)} %dynamic-update-slice), channel_id=4, replica_groups=mesh['sp_0'=8,'sp_1'=4,'tp_0'=8,'tp_1'=2] {'sp_1'}, use_global_device_ids=true, to_apply=%add.1 | all-reduce | flops 32 | bytes 128
  31.1 22.0 %all_gather.46 = bf16[8,1,4]{2,1,0:T(2,128)(2,1)S(1)} all-gather(bf16[1,1,4]{2,1,0:T(2,128)(2,1)S(1)} %get-tuple-element.265), channel_id=1, replica_groups=mesh['sp_0'=8,'sp_1'=4,'tp_0'=8,'tp_1'=2] {'sp_0'}, dimensions={0}, use_global_device_ids=true | all-gather | bytes 72 | tf_op jit(solution)/shard_map/all_gather | solution.py:48
  53.8 13.3 %all_gather.51 = bf16[8,1,4]{2,1,0:T(2,128)(2,1)S(1)} all-gather(bf16[1,1,4]{2,1,0:T(2,128)(2,1)S(1)} %get-tuple-element.269), channel_id=1, replica_groups=mesh['sp_0'=8,'sp_1'=4,'tp_0'=8,'tp_1'=2] {'sp_0'}, dimensions={0}, use_global_device_ids=true | all-gather | bytes 72 | tf_op jit(solution)/shard_map/all_gather | solution.py:48
  76.0 12.3 %all-gather.1 = bf16[4,4,64,128]{3,2,1,0:T(8,128)(2,1)S(1)} all-gather(bf16[1,4,64,128]{3,2,1,0:T(8,128)(2,1)S(1)} %convert_element_type.652), channel_id=3, replica_groups=mesh['sp_0'=8,'sp_1'=4,'tp_0'=8,'tp_1'=2] {'sp_1'}, dimensions={0}, use_global_device_ids=true | all-gather | bytes 327680 | tf_op jit(solution)/shard_map/all_gather | solution.py:48
  88.4 25.2 %all_gather.49 = bf16[8,1,4,64,128]{4,3,2,1,0:T(8,128)(2,1)S(1)} all-gather(bf16[1,1,4,64,128]{4,3,2,1,0:T(8,128)(2,1)S(1)} %fusion.75), channel_id=1, replica_groups=mesh['sp_0'=8,'sp_1'=4,'tp_0'=8,'tp_1'=2] {'sp_0'}, dimensions={0}, use_global_device_ids=true | all-gather | bytes 589824 | tf_op jit(solution)/shard_map/all_gather | solution.py:48
  115.6 12.3 %all-gather.3 = bf16[4,4,64,128]{3,2,1,0:T(8,128)(2,1)S(1)} all-gather(bf16[1,4,64,128]{3,2,1,0:T(8,128)(2,1)S(1)} %convert_element_type.683), channel_id=5, replica_groups=mesh['sp_0'=8,'sp_1'=4,'tp_0'=8,'tp_1'=2] {'sp_1'}, dimensions={0}, use_global_device_ids=true | all-gather | bytes 327680 | tf_op jit(solution)/shard_map/all_gather | solution.py:48
  128.0 25.2 %all_gather.54 = bf16[8,1,4,64,128]{4,3,2,1,0:T(8,128)(2,1)S(1)} all-gather(bf16[1,1,4,64,128]{4,3,2,1,0:T(8,128)(2,1)S(1)} %fusion.72), channel_id=1, replica_groups=mesh['sp_0'=8,'sp_1'=4,'tp_0'=8,'tp_1'=2] {'sp_0'}, dimensions={0}, use_global_device_ids=true | all-gather | bytes 589824 | tf_op jit(solution)/shard_map/all_gather | solution.py:48
  163.0 2.1 all_gather.55
  166.5 40.7 %all-gather.8.cloned.1.call-done = bf16[256,4096]{0,1:T(8,128)(2,1)} async-done(((bf16[256,512]{0,1:T(8,128)(2,1)}), bf16[256,4096]{0,1:T(8,128)(2,1)}) %all-gather.8.cloned.1.call-update) | async-done | bytes 2097168 | tf_op jit(solution)/shard_map/all_gather | solution.py:66
  207.2 3.2 convolution_convert_fusion.2
  210.4 4.3 %all-to-all-start = ((bf16[16,16,128]{2,1,0:T(8,128)(2,1)}), bf16[16,16,128]{2,1,0:T(8,128)(2,1)S(1)}, u32[]{:S(2)}, u32[]{:S(2)}) async-start(bf16[16,16,128]{2,1,0:T(8,128)(2,1)} %bitcast.67), calls=%async_computation | async-start | bytes 131072 | tf_op jit(solution)/shard_map/all_to_all | solution.py:260
  214.9 7.6 %all-to-all-done = bf16[16,16,128]{2,1,0:T(8,128)(2,1)S(1)} async-done(((bf16[16,16,128]{2,1,0:T(8,128)(2,1)}), bf16[16,16,128]{2,1,0:T(8,128)(2,1)S(1)}, u32[]{:S(2)}, u32[]{:S(2)}) %all-to-all-start) | async-done | bytes 65568 | tf_op jit(solution)/shard_map/all_to_all | solution.py:260
  223.1 22.2 %all_to_all.23 = bf16[32,2,2048]{2,1,0:T(2,128)(2,1)} all-to-all(bf16[32,2,2048]{2,1,0:T(2,128)(2,1)S(1)} %reshape.1011), channel_id=1, replica_groups=mesh['sp_0'=8,'sp_1'=4,'tp_0'=8,'tp_1'=2] {'sp_0','sp_1'}, dimensions={0} | all-to-all | bytes 524288 | tf_op jit(solution)/shard_map/all_to_all | solution.py:280
  245.6 36.0 %all-gather.10.cloned.1.call-done = bf16[512,2,2048]{2,1,0:T(2,128)(2,1)} async-done(((bf16[32,2,2048]{2,1,0:T(2,128)(2,1)}), bf16[512,2,2048]{2,1,0:T(2,128)(2,1)}) %all-gather.10.cloned.1.call-update) | async-done | bytes 4194320 | tf_op jit(solution)/shard_map/all_gather | solution.py:287
  281.6 7.2 %reshape.1012 = bf16[1024,2048]{1,0:T(8,128)(2,1)} reshape(bf16[512,2,2048]{2,1,0:T(2,128)(2,1)} %all-gather.10.cloned.1.call-done) | data formatting | bytes 8388608 | tf_op jit(solution)/shard_map/reshape | solution.py:288
  288.8 4.5 %fusion.14 = f32[1024,256]{1,0:T(8,128)} fusion(bf16[1024,2048]{1,0:T(8,128)(2,1)} %reshape.1012, bf16[1,2048,256]{2,1,0:T(8,128)(2,1)S(1)} %copy-done.16), kind=kOutput, calls=%fused_computation.31 | convolution fusion | flops 1073741824 | bytes 6291456 | tf_op jit(solution)/shard_map/dot_general | solution.py:289
  293.3 9.1 %convolution_convert_fusion = bf16[1024,2048]{1,0:T(8,128)(2,1)} fusion(bf16[1024,2048]{1,0:T(8,128)(2,1)} %reshape.1012, bf16[1,256,2048]{2,1,0:T(8,128)(2,1)S(1)} %copy-done, bf16[1,2048,256]{2,1,0:T(8,128)(2,1)} %param.40, f32[1024,256]{1,0:T(8,128)} %fusion.14), kind=kOutput, calls=%fused_computation.10 | convolution fusion | flops 2151153664 | bytes 11534336 | tf_op jit(solution)/shard_map/dot_general | solution.py:292
  302.4 7.6 %convert_element_type.713 = bf16[16,32,2,2048]{3,2,1,0:T(2,128)(2,1)} reshape(bf16[1024,2048]{1,0:T(8,128)(2,1)} %convolution_convert_fusion) | data formatting | bytes 8388608 | tf_op jit(solution)/shard_map/convert_element_type | solution.py:296
  310.1 6.1 %copy.156 = bf16[16,32,2,2048]{3,1,2,0:T(8,128)(2,1)} copy(bf16[16,32,2,2048]{3,2,1,0:T(2,128)(2,1)} %convert_element_type.713) | data formatting | bytes 8388608 | tf_op jit(solution)/shard_map/convert_element_type | solution.py:296
  316.1 64.6 %reduce-scatter.2.cloned.1.call-done = bf16[1,32,2,2048]{3,1,2,0:T(8,128)(2,1)} async-done(((bf16[16,32,2,2048]{3,1,2,0:T(8,128)(2,1)}), bf16[1,32,2,2048]{3,1,2,0:T(8,128)(2,1)}) %reduce-scatter.2.cloned.1.call-update) | async-done | bytes 262160 | tf_op jit(solution)/shard_map/reduce_scatter | solution.py:295
  382.7 10.5 %all-to-all-start.2 = ((bf16[32,2,2048]{2,1,0:T(2,128)(2,1)}), bf16[32,2,2048]{2,1,0:T(2,128)(2,1)S(1)}, u32[]{:S(2)}, u32[]{:S(2)}) async-start(bf16[32,2,2048]{2,1,0:T(2,128)(2,1)} %copy.157), calls=%async_computation.3 | async-start | bytes 524288 | tf_op jit(solution)/shard_map/all_to_all | solution.py:302
  393.3 9.8 %all-to-all-done.2 = bf16[32,2,2048]{2,1,0:T(2,128)(2,1)S(1)} async-done(((bf16[32,2,2048]{2,1,0:T(2,128)(2,1)}), bf16[32,2,2048]{2,1,0:T(2,128)(2,1)S(1)}, u32[]{:S(2)}, u32[]{:S(2)}) %all-to-all-start.2) | async-done | bytes 262176 | tf_op jit(solution)/shard_map/all_to_all | solution.py:302
  (142 shorter events, 36.7 us)
Async XLA Ops:
  6.5 286.8 %copy-start = (bf16[1,256,2048]{2,1,0:T(8,128)(2,1)S(1)}, bf16[1,256,2048]{2,1,0:T(8,128)(2,1)}, u32[]{:S(2)}) copy-start(bf16[1,256,2048]{2,1,0:T(8,128)(2,1)} %param.41) | copy-start | bytes 3145732
  6.5 200.6 %all-gather.8.cloned.1.call-start = ((), (), s32[]{:S(2)}) async-start(), calls=%async_computation.4 | async-start | bytes 2359296 | tf_op jit(solution)/shard_map/all_gather | solution.py:66
  9.7 62.9 %collective-permute-start = (bf16[2,512]{0,1:T(8,128)(2,1)S(1)}, bf16[2,512]{0,1:T(8,128)(2,1)S(1)}, u32[]{:S(2)}, u32[]{:S(2)}) collective-permute-start(bf16[2,512]{0,1:T(8,128)(2,1)S(1)} %get-tuple-element.275), channel_id=1, source_target_pairs={{0,16},{16,32},{32,48},{48,64},{64,80},{80,96},{96,112},{112,128},... | collective-permute-start | bytes 6152 | tf_op jit(solution)/shard_map/ppermute | solution.py:27
  13.9 58.8 %collective-permute-start.1 = (bf16[2,512]{0,1:T(8,128)(2,1)S(1)}, bf16[2,512]{0,1:T(8,128)(2,1)S(1)}, u32[]{:S(2)}, u32[]{:S(2)}) collective-permute-start(bf16[2,512]{0,1:T(8,128)(2,1)S(1)} %get-tuple-element.276), channel_id=1, source_target_pairs={{16,0},{32,16},{48,32},{64,48},{80,64},{96,80},{112,96},{128,112},... | collective-permute-start | bytes 6152 | tf_op jit(solution)/shard_map/ppermute | solution.py:29
  19.5 53.0 %copy-start.5 = (f32[2,4]{1,0:T(2,128)}, f32[2,4]{1,0:T(2,128)S(1)}, u32[]{:S(2)}) copy-start(f32[2,4]{1,0:T(2,128)S(1)} %get-tuple-element.240) | copy-start | bytes 100
  70.8 17.5 %copy-start.7 = (f32[4]{0:T(128)}, f32[4]{0:T(128)S(1)}, u32[]{:S(2)}) copy-start(f32[4]{0:T(128)S(1)} %get-tuple-element.308) | copy-start | bytes 52
  70.8 17.5 %copy-start.8 = (f32[4]{0:T(128)}, f32[4]{0:T(128)S(1)}, u32[]{:S(2)}) copy-start(f32[4]{0:T(128)S(1)} %get-tuple-element.309) | copy-start | bytes 52
  70.8 17.5 %copy-start.9 = (f32[4]{0:T(128)}, f32[4]{0:T(128)S(1)}, u32[]{:S(2)}) copy-start(f32[4]{0:T(128)S(1)} %get-tuple-element.310) | copy-start | bytes 52
  70.8 17.5 %copy-start.10 = (f32[4]{0:T(128)}, f32[4]{0:T(128)S(1)}, u32[]{:S(2)}) copy-start(f32[4]{0:T(128)S(1)} %get-tuple-element.311) | copy-start | bytes 52
  74.9 0.6 copy-start.2
  75.6 52.3 %copy-start.11 = (f32[4]{0:T(128)S(1)}, f32[4]{0:T(128)}, u32[]{:S(2)}) copy-start(f32[4]{0:T(128)} %get-tuple-element.313) | copy-start | bytes 52
  75.6 52.2 %copy-start.12 = (f32[4]{0:T(128)S(1)}, f32[4]{0:T(128)}, u32[]{:S(2)}) copy-start(f32[4]{0:T(128)} %get-tuple-element.314) | copy-start | bytes 52
  75.6 52.2 %copy-start.13 = (f32[4]{0:T(128)S(1)}, f32[4]{0:T(128)}, u32[]{:S(2)}) copy-start(f32[4]{0:T(128)} %get-tuple-element.315) | copy-start | bytes 52
  75.6 52.2 %copy-start.14 = (f32[4]{0:T(128)S(1)}, f32[4]{0:T(128)}, u32[]{:S(2)}) copy-start(f32[4]{0:T(128)} %get-tuple-element.316) | copy-start | bytes 52
  75.9 38.1 %copy-start.1 = (f32[2,1,4,64,128]{4,3,2,1,0:T(8,128)}, f32[2,1,4,64,128]{4,3,2,1,0:T(8,128)S(1)}, u32[]{:S(2)}) copy-start(f32[2,1,4,64,128]{4,3,2,1,0:T(8,128)S(1)} %get-tuple-element.138) | copy-start | bytes 786436
  113.7 14.2 %copy-start.3 = (bf16[2,128,4,64]{1,0,3,2:T(2,128)(2,1)}, bf16[2,128,4,64]{1,0,3,2:T(2,128)(2,1)S(1)}, u32[]{:S(2)}) copy-start(bf16[2,128,4,64]{1,0,3,2:T(2,128)(2,1)S(1)} %reshape.1006) | copy-start | bytes 393220
  158.7 63.8 %copy-start.4 = (bf16[16,2048]{1,0:T(8,128)(2,1)S(1)}, bf16[16,2048]{1,0:T(8,128)(2,1)}, u32[]{:S(2)}) copy-start(bf16[16,2048]{1,0:T(8,128)(2,1)} %param.23) | copy-start | bytes 196612
  158.7 63.9 %copy-start.6 = (f32[2048]{0:T(1024)S(1)}, f32[2048]{0:T(1024)}, u32[]{:S(2)}) copy-start(f32[2048]{0:T(1024)} %param.36) | copy-start | bytes 24580
  210.4 12.1 %all-to-all-start = ((bf16[16,16,128]{2,1,0:T(8,128)(2,1)}), bf16[16,16,128]{2,1,0:T(8,128)(2,1)S(1)}, u32[]{:S(2)}, u32[]{:S(2)}) async-start(bf16[16,16,128]{2,1,0:T(8,128)(2,1)} %bitcast.67), calls=%async_computation | async-start | bytes 131072 | tf_op jit(solution)/shard_map/all_to_all | solution.py:260
  214.7 66.9 %all-gather.10.cloned.1.call-start = ((), (), s32[]{:S(2)}) async-start(), calls=%async_computation.6 | async-start | bytes 4456448 | tf_op jit(solution)/shard_map/all_gather | solution.py:287
  245.3 43.5 %copy-start.16 = (bf16[1,2048,256]{2,1,0:T(8,128)(2,1)S(1)}, bf16[1,2048,256]{2,1,0:T(8,128)(2,1)}, u32[]{:S(2)}) copy-start(bf16[1,2048,256]{2,1,0:T(8,128)(2,1)} %param.39) | copy-start | bytes 3145732
  245.4 135.4 %reduce-scatter.2.cloned.1.call-start = ((), (), s32[]{:S(2)}) async-start(), calls=%async_computation.5 | async-start | bytes 4456448 | tf_op jit(solution)/shard_map/reduce_scatter | solution.py:295
  316.1 77.1 %copy-start.15 = (f32[16,2]{0,1:T(2,128)S(1)}, f32[16,2]{0,1:T(2,128)}, u32[]{:S(2)}) copy-start(f32[16,2]{0,1:T(2,128)} %param.38) | copy-start | bytes 388
  382.7 20.4 %all-to-all-start.2 = ((bf16[32,2,2048]{2,1,0:T(2,128)(2,1)}), bf16[32,2,2048]{2,1,0:T(2,128)(2,1)S(1)}, u32[]{:S(2)}, u32[]{:S(2)}) async-start(bf16[32,2,2048]{2,1,0:T(2,128)(2,1)} %copy.157), calls=%async_computation.3 | async-start | bytes 524288 | tf_op jit(solution)/shard_map/all_to_all | solution.py:302
Sparse Core Ops, SparseCore 0:
  165.3 41.8 all-gather.7
  245.5 36.1 all-gather.9
  316.3 64.4 reduce-scatter.1
where the time goes:
time: 413 us; the launch traced here: 411 us
  waiting for transfers between devices  159 us (38%)
  blocking collectives  144 us (35%)
  local copies, waits for them, and re-layouts  35.1 us (8%)
  matrix products  23.8 us (6%)
  starting transfers between devices  21.2 us (5%)
  between operations  14.4 us (3%)
  other arithmetic  13.4 us (3%)
    all_gather x6, blocking collectives, carried_in(): lax.all_gather(part.astype(kind), axis)  110 us
    reduce_scatter x1, waiting for transfers between devices, shards(): lax.psum_scatter(partial_sum.astype(jnp.float32).reshape(arrived.shape).a...  64.6 us
    all_gather x1, waiting for transfers between devices, gather_axes(): filled = lax.all_gather(filled, axes[number], axis=dim, tiled=True)  40.7 us
    all_gather x1, waiting for transfers between devices, shards(): arrived = lax.all_gather(received[None], TP, axis=0, tiled=True)  36 us
    all_to_all x1, blocking collectives, shards(): lax.all_to_all(outgoing.reshape(experts, capacity, model_width), SP, spli...  22.2 us
    convert_element_type x2, local copies, waits for them, and re-layouts, shards(): partial_sum.astype(jnp.float32).reshape(arrived.shape).astype(jnp.bfloat16)  13.7 us
    all_to_all x1, starting transfers between devices, shards(): lax.all_to_all(results, SP, split_axis=0, concat_axis=0, tiled=True)  10.5 us
    all_to_all x1, waiting for transfers between devices, shards(): lax.all_to_all(results, SP, split_axis=0, concat_axis=0, tiled=True)  9.83 us
  transfers between devices with their start and end apart: 7, of which 5 were waited for; matrix products, arithmetic and copies ran while one was open for 3% of the time, Pallas kernels for 0%

commit v1 on v0

v1 whole, which is shorter than its diff:
```python
import functools

import jax
import jax.numpy as jnp
from jax import lax
from jax.experimental import pallas as pl
from jax.experimental.pallas import tpu as pltpu
from jax.sharding import PartitionSpec as P

MESH = pl.DeviceIdType.MESH
HIGH = lax.Precision.HIGHEST
F32 = jnp.float32
BF16 = jnp.bfloat16
EPS = 1e-06
BLOCK = 128
NCH = 4


def dot(a, b, contract=((1,), (0,)), precision=None):
    return lax.dot_general(
        a, b, (contract, ((), ())), preferred_element_type=F32, precision=precision
    )


def silu(v):
    return v / (1.0 + jnp.exp(-v))


def rcopy(src, dst, send, recv, dev):
    return pltpu.make_async_remote_copy(
        src_ref=src, dst_ref=dst, send_sem=send, recv_sem=recv, device_id=dev, device_id_type=MESH
    )


def wait_bytes(ref, sem):
    pltpu.make_async_copy(ref, ref, sem).wait()


def iota(shape, dim):
    return lax.broadcasted_iota(jnp.int32, shape, dim)


def body(
    nsp,
    ntp,
    resid,
    v_in,
    k_in,
    q_in,
    og_in,
    raw_in,
    extra_in,
    rate_in,
    vf_in,
    kf_in,
    qf_in,
    gain_in,
    wout,
    ngain_in,
    routes_in,
    cw_in,
    wg,
    wu,
    wd,
    out,
    hl,
    hr,
    pad,
    tot_s,
    tot_r,
    st_s,
    st_r,
    sc_f,
    sc_s,
    sc_r,
    heads,
    wc,
    po,
    mo,
    dm,
    dr,
    rowsf,
    xs,
    wgu,
    wdn,
    acc,
    zs,
    sp_b,
    sn_b,
    rp_b,
    rn_b,
    bm,
    br,
    lsem,
    hsem,
    tsem,
    ssem,
    osem,
    hdsem,
    wsem,
    swsem,
    psem,
    dsem,
    ag_send,
    ag_recv,
    rs_send,
    rs_recv,
    bsem,
):
    me = lax.axis_index("sp")
    tp = lax.axis_index("tp")
    ny = ntp // 2
    y = tp // 2
    c = tp % 2
    partner = y * 2 + (1 - c)
    right_y = ((y + 1) % ny) * 2 + c
    left_y = ((y + ny - 1) % ny) * 2 + c
    others = nsp - 1

    bar = pltpu.get_barrier_semaphore()

    @pl.loop(1, nsp)
    def _(i):
        pl.semaphore_signal(bar, inc=1, device_id={"sp": (me + i) % nsp}, device_id_type=MESH)

    @pl.loop(1, ntp)
    def _(i):
        pl.semaphore_signal(bar, inc=1, device_id={"tp": (tp + i) % ntp}, device_id_type=MESH)

    ff = wg.shape[1]
    chan = wout.shape[0] // ny
    ycol = pl.ds(pl.multiple_of(y * 128, 128), 128)
    loads = [
        pltpu.make_async_copy(wout.at[pl.ds(pl.multiple_of(y * chan, chan), chan)], wc.at[:, ycol], lsem.at[0]),
        pltpu.make_async_copy(wg, wgu.at[:, pl.ds(0, ff)], lsem.at[1]),
        pltpu.make_async_copy(wu, wgu.at[:, pl.ds(2 * ff, ff)], lsem.at[2]),
        pltpu.make_async_copy(wd, wdn.at[pl.ds(0, ff)], lsem.at[3]),
    ]
    for load in loads:
        load.start()

    lane = iota((1, 128), 1)
    step8 = raw_in[...]
    step8 = jnp.maximum(step8, 0.0) + jnp.log1p(jnp.exp(-jnp.abs(step8)))
    log8 = rate_in[...] * step8 + extra_in[...]
    row = iota((BLOCK, BLOCK), 0)
    col = iota((BLOCK, BLOCK), 1)
    lower = (col <= row).astype(F32)
    ones = jnp.ones((BLOCK, BLOCK), F32)
    spread = ((iota((128, 512), 1) // 64) == iota((128, 512), 0)).astype(F32)
    cum, cum_t, tot_c, sw8, rd8 = [], [], [], [], []
    for b in range(2):
        logs = log8[b * BLOCK : (b + 1) * BLOCK]
        run = dot(lower, logs, precision=HIGH)
        total = run[BLOCK - 1 : BLOCK]
        both = run - jnp.where(lane >= 4, logs, 0.0)
        cum.append(both)
        cum_t.append(both.T)
        tot_c.append(dot(logs, ones, ((0,), (0,)), HIGH)[0:8])
        sw8.append(jnp.exp(jnp.where(lane < 4, total - both, both)))
        rd8.append(jnp.exp(jnp.where(lane < 4, both, total - both)))
    tot_dev = jnp.exp(tot_c[0] + tot_c[1])
    tot_s[...] = tot_dev
    tot_r[me] = tot_dev
    step_x = dot(step8, spread, precision=HIGH)
    sw_x = [dot(sw8[b], spread, precision=HIGH) for b in range(2)]
    rd_x = [dot(rd8[b], spread, precision=HIGH) for b in range(2)]

    def head_rows(b, first):
        e = jnp.exp(tot_c[b][first : first + 4])
        return jnp.concatenate([jnp.broadcast_to(e[h : h + 1], (64, 128)) for h in range(4)], axis=0)

    pl.semaphore_wait(bar, nsp - 1 + ntp - 1)

    right = {"sp": (me + 1) % nsp}
    left = {"sp": (me + nsp - 1) % nsp}
    tokens = v_in.shape[0]
    for ref, lo, width in ((v_in, 0, 256), (k_in, 256, 128), (q_in, 384, 128)):
        cols = pl.ds(lo, width)
        rcopy(ref.at[pl.ds(tokens - 16, 16)], hl.at[:, cols], hsem.at[0], hsem.at[1], right).start()
        rcopy(ref.at[pl.ds(0, 16)], hr.at[:, cols], hsem.at[2], hsem.at[3], left).start()

    @pl.loop(1, nsp)
    def _(i):
        rcopy(tot_s, tot_r.at[me], tsem.at[0], tsem.at[1], {"sp": (me + i) % nsp}).start()

    @pl.loop(1, ny)
    def _(i):
        dst = (y + i) % ny
        rcopy(
            wout.at[pl.ds(pl.multiple_of(dst * chan, chan), chan)],
            wc.at[:, ycol],
            wsem.at[0],
            wsem.at[1],
            {"tp": dst * 2 + c},
        ).start()

    swaps = [
        rcopy(wg, wgu.at[:, pl.ds(ff, ff)], swsem.at[0], swsem.at[1], {"tp": partner}),
        rcopy(wu, wgu.at[:, pl.ds(3 * ff, ff)], swsem.at[2], swsem.at[3], {"tp": partner}),
        rcopy(wd, wdn.at[pl.ds(ff, ff)], swsem.at[4], swsem.at[5], {"tp": partner}),
    ]
    for swap in swaps:
        swap.start()

    pad[16 : 16 + tokens, 0:256] = v_in[...].astype(F32)
    pad[16 : 16 + tokens, 256:384] = k_in[...].astype(F32)
    pad[16 : 16 + tokens, 384:512] = q_in[...].astype(F32)
    wait_bytes(hl, hsem.at[1])
    wait_bytes(hr, hsem.at[3])
    pad[0:16] = jnp.where(me > 0, hl[...].astype(F32), 0.0)
    pad[16 + tokens : 32 + tokens] = jnp.where(me < nsp - 1, hr[...].astype(F32), 0.0)
    filt = jnp.concatenate([vf_in[...], kf_in[...], qf_in[...]], axis=1).astype(F32)
    conv = filt[0:1] * pad[14 : 14 + tokens]
    for o in range(1, 5):
        conv = conv + filt[o : o + 1] * pad[14 + o : 14 + o + tokens]
    values = conv[:, 0:256].astype(BF16).astype(F32)
    keys = silu(conv[:, 256:384]).astype(BF16)
    queries = silu(conv[:, 384:512]).astype(BF16)
    scaled = (jnp.concatenate([values, values], axis=1) * step_x).astype(BF16)

    part = []
    for b in range(2):
        rows = slice(b * BLOCK, (b + 1) * BLOCK)
        weighted = (scaled[rows].astype(F32) * sw_x[b]).astype(BF16)
        part.append(dot(weighted, keys[rows], ((0,), (0,))))
    final_f = head_rows(1, 0) * part[0][0:256] + part[1][0:256]
    final_b = head_rows(0, 4) * part[1][256:512] + part[0][256:512]
    piece = 256 // nsp
    mine = jnp.concatenate(
        [final_f.reshape(nsp, piece, 128), final_b.reshape(nsp, piece, 128)], axis=1
    ).astype(BF16)
    st_s[...] = mine

    @pl.loop(1, nsp)
    def _(i):
        dst = (me + i) % nsp
        rcopy(st_s.at[dst], st_r.at[me], ssem.at[0], ssem.at[1], {"sp": dst}).start()

    st_r[me] = st_s[me]

    inner = []
    lo_half = lane < 64
    for b in range(2):
        rows = slice(b * BLOCK, (b + 1) * BLOCK)
        score = dot(queries[rows], keys[rows], ((1,), (1,)))
        pairs = []
        for pair in range(2):
            halves = []
            for h in (2 * pair, 2 * pair + 1):
                f_gap = cum[b][:, h : h + 1] - cum_t[b][h : h + 1, :]
                b_gap = cum_t[b][4 + h : 5 + h, :] - cum[b][:, 4 + h : 5 + h]
                w = score * jnp.exp(jnp.where(col <= row, f_gap, b_gap))
                w_f = jnp.where(col <= row, w, 0.0)
                w_b = jnp.where(col >= row, w, 0.0)
                both = jnp.concatenate([w_f, w_b], axis=1).astype(BF16)
                lanes = slice(128 * pair, 128 * pair + 128)
                rhs = jnp.concatenate(
                    [scaled[rows, lanes], scaled[rows, 256 + 128 * pair : 384 + 128 * pair]], axis=0
                )
                halves.append(dot(both, rhs))
            pairs.append(jnp.where(lo_half, halves[0], halves[1]))
        inner.append(jnp.concatenate(pairs, axis=1))
    gate_act = silu(og_in[...].astype(F32))

    own = routes_in.shape[0] // ntp
    my_routes = routes_in[pl.ds(pl.multiple_of(tp * own, own), own), :]
    e_lane = iota((own, 128), 1)
    hot0 = (my_routes[:, 0:1] == e_lane).astype(F32)
    hot1 = (my_routes[:, 1:2] == e_lane).astype(F32)
    strict = (iota((own, own), 1) < iota((own, own), 0)).astype(F32)
    before = dot(strict, hot0 + hot1, precision=HIGH)
    ids = e_lane.astype(F32) * 2.0 + before
    slot0 = jnp.sum(hot0 * ids, axis=1, keepdims=True)
    slot1 = jnp.sum(hot1 * ids, axis=1, keepdims=True)
    r_id = iota((NCH * own, nsp * 8), 1)
    r_slot = ((r_id // 8) * 2 + r_id % 2).astype(F32)
    same = ((r_id // 2) % 4) == (iota((NCH * own, nsp * 8), 0) // own)
    hit0 = same & (r_slot == jnp.concatenate([slot0] * NCH, axis=0))
    hit1 = same & (r_slot == jnp.concatenate([slot1] * NCH, axis=0))
    place = jnp.where(hit0 | hit1, 1.0, 0.0).astype(BF16)
    w0 = jnp.concatenate([cw_in[:, 0:1]] * NCH, axis=0)
    w1 = jnp.concatenate([cw_in[:, 1:2]] * NCH, axis=0)
    mixing = jnp.where(hit0, w0, 0.0) + jnp.where(hit1, w1, 0.0)
    mix_hi = mixing.astype(BF16)
    mix_lo = (mixing - mix_hi.astype(F32)).astype(BF16)

    wait_bytes(tot_r.at[pl.ds(0, others)], tsem.at[1])
    wait_bytes(st_r.at[pl.ds(0, others)], ssem.at[1])
    head = me // (64 // piece)

    def forward(d, carry):
        sc_f[d, 0:piece] = carry
        decay = tot_r[d, pl.ds(head, 1), :]
        return decay * carry + st_r[d].astype(F32)[0:piece]

    def backward(i, carry):
        d = nsp - 1 - i
        sc_f[d, piece : 2 * piece] = carry
        decay = tot_r[d, pl.ds(head + 4, 1), :]
        return decay * carry + st_r[d].astype(F32)[piece : 2 * piece]

    zero = jnp.zeros((piece, 128), F32)
    lax.fori_loop(0, nsp, forward, zero)
    lax.fori_loop(0, nsp, backward, zero)
    sc_s[...] = sc_f[...].astype(BF16)

    @pl.loop(1, nsp)
    def _(i):
        dst = (me + i) % nsp
        rcopy(sc_s.at[dst], sc_r.at[me], osem.at[0], osem.at[1], {"sp": dst}).start()

    sc_r[me] = sc_s[me]
    wait_bytes(sc_r.at[pl.ds(0, others)], osem.at[1])

    around = sc_r[...].astype(F32)
    enter = around[:, 0:piece].reshape(256, 128)
    leave = around[:, piece : 2 * piece].reshape(256, 128)
    enters = [enter, head_rows(0, 0) * enter + part[0][0:256]]
    leaves = [head_rows(1, 4) * leave + part[1][256:512], leave]
    group = (iota((256, 256), 0) // 64 == iota((256, 256), 1) // 64).astype(F32) * (1.0 / 64.0)
    for b in range(2):
        rows = slice(b * BLOCK, (b + 1) * BLOCK)
        state = jnp.concatenate([enters[b], leaves[b]], axis=0).astype(BF16)
        read = dot(queries[rows], state, ((1,), (1,))) * rd_x[b]
        gated = (inner[b] + read[:, 0:256] + read[:, 256:512]) * gate_act[rows]
        mean = dot(gated * gated, group, precision=HIGH)
        normed = gated * lax.rsqrt(mean + EPS) * gain_in[...]
        heads[c, rows, :] = normed.astype(BF16)

    swap_h = rcopy(heads.at[c], heads.at[c], hdsem.at[0], hdsem.at[1], {"tp": partner})
    swap_h.start()

    loads[0].wait()
    wait_bytes(wc.at[:, pl.ds(0, 128 * (ny - 1))], wsem.at[1])
    inner_c = chan // 2
    own_part = dot(heads[c], wc[pl.ds(pl.multiple_of(c * inner_c, inner_c), inner_c), :])
    swap_h.wait()
    o_c = 1 - c
    full = own_part + dot(heads[o_c], wc[pl.ds(pl.multiple_of(o_c * inner_c, inner_c), inner_c), :])
    po[...] = full.reshape(ntp, own, full.shape[1]).astype(BF16)

    @pl.loop(1, ntp)
    def _(i):
        dst = (tp + i) % ntp
        rcopy(po.at[dst], mo.at[tp], psem.at[0], psem.at[1], {"tp": dst}).start()

    mo[tp] = po[tp]
    wait_bytes(mo.at[pl.ds(0, ntp - 1)], psem.at[1])
    halves = []
    for core in range(2):
        total = mo[core].astype(F32)
        for other in range(1, ny):
            total = total + mo[2 * other + core].astype(F32)
        halves.append(total)
    pieces = []
    for j in range(ny):
        pieces += [halves[0][:, 128 * j : 128 * j + 128], halves[1][:, 128 * j : 128 * j + 128]]
    mixer_out = jnp.concatenate(pieces, axis=1).astype(BF16).astype(F32)
    middle = (resid[...].astype(F32) + mixer_out).astype(BF16).astype(F32)
    square = jnp.mean(middle * middle, axis=-1, keepdims=True)
    normed = (middle * lax.rsqrt(square + EPS) * ngain_in[...]).astype(BF16)
    width = normed.shape[1] // NCH
    stacked = jnp.concatenate([normed[:, j * width : (j + 1) * width] for j in range(NCH)], axis=0)
    sent = dot(place, stacked, ((0,), (0,)))
    dm[...] = sent.reshape(nsp, 8, width).astype(BF16)

    @pl.loop(1, nsp)
    def _(i):
        dst = (me + i) % nsp
        rcopy(dm.at[dst], dr.at[me], dsem.at[0], dsem.at[1], {"sp": dst}).start()

    dr[me] = dm[me]
    wait_bytes(dr.at[pl.ds(0, others)], dsem.at[1])
    arrived = dr[...].astype(F32).reshape(nsp * 8, width)
    for n in range(width // 128):
        rowsf[n] = arrived[:, n * 128 : (n + 1) * 128]
    r_dev = {"tp": right_y}
    l_dev = {"tp": left_y}
    for j in range(NCH):
        for s in range(2):
            for n in range(width // 128):
                picked = rowsf[n, pl.ds(2 * j + s, nsp, stride=8), :]
                xs[0, j, s * nsp : (s + 1) * nsp, n * 128 : (n + 1) * 128] = picked.astype(BF16)
        rcopy(xs.at[0, j], xs.at[1, j], ag_send.at[0, 0], ag_recv.at[0, 1, j], r_dev).start()
        rcopy(xs.at[0, j], xs.at[5, j], ag_send.at[1, 0], ag_recv.at[1, 1, j], l_dev).start()

    for load in loads[1:]:
        load.wait()
    for swap in swaps:
        swap.wait()

    rows1 = 2 * nsp

    def add_chunk(x, j, first):
        n = x.shape[0]
        w = wgu[pl.ds(pl.multiple_of(j * width, width), width), :]
        g = dot(x, w)

        @pl.when(first)
        def _():
            acc[0:n] = g

        @pl.when(jnp.logical_not(first))
        def _():
            acc[0:n] += g

    def finish(n, store):
        g = acc[0:n, 0 : 2 * ff]
        u = acc[0:n, 2 * ff : 4 * ff]
        hidden = (silu(g) * u).astype(BF16)
        for j in range(NCH):
            store(j, dot(hidden, wdn[:, j * width : (j + 1) * width]))

    def store_own(j, z):
        zs[0, j] = z

    @pl.loop(0, NCH)
    def _(j):
        add_chunk(xs[0, j], j, j == 0)

    finish(rows1, store_own)

    @pl.loop(0, 3 * NCH)
    def _(t):
        k = 1 + t // NCH
        j = t % NCH
        wait_bytes(xs.at[k, j], ag_recv.at[0, k, j])
        wait_bytes(xs.at[4 + k, j], ag_recv.at[1, k, j])

        @pl.when(k < 3)
        def _():
            rcopy(xs.at[k, j], xs.at[k + 1, j], ag_send.at[0, k], ag_recv.at[0, k + 1, j], r_dev).start()
            rcopy(xs.at[4 + k, j], xs.at[5 + k, j], ag_send.at[1, k], ag_recv.at[1, k + 1, j], l_dev).start()

        @pl.when((k == 3) & (j < 2))
        def _():
            rcopy(xs.at[3, j], xs.at[4, j], ag_send.at[0, 3], ag_recv.at[0, 4, j], r_dev).start()

        @pl.when((k == 3) & (j >= 2))
        def _():
            rcopy(xs.at[7, j], xs.at[4, j], ag_send.at[1, 3], ag_recv.at[1, 4, j], l_dev).start()

        add_chunk(jnp.concatenate([xs[k, j], xs[4 + k, j]], axis=0), j, j == 0)

        @pl.when(j == NCH - 1)
        def _():
            def store(i, z):
                zs[k, i] = z[0:rows1]
                zs[4 + k, i] = z[rows1 : 2 * rows1]

            finish(2 * rows1, store)

    for j in (0, 2, 1, 3):
        wait_bytes(xs.at[4, j], ag_recv.at[0 if j < 2 else 1, 4, j])
        add_chunk(xs[4, j], j, j == 0)

    def store_far(j, z):
        zs[4, j] = z
        if j < 2:
            sp_b[3, j] = z.astype(BF16)
            rcopy(sp_b.at[3, j], rp_b.at[3, j], rs_send.at[0, 3], rs_recv.at[0, 3, j], r_dev).start()
        else:
            sn_b[3, j] = z.astype(BF16)
            rcopy(sn_b.at[3, j], rn_b.at[3, j], rs_send.at[1, 3], rs_recv.at[1, 3, j], l_dev).start()

    finish(rows1, store_far)

    @pl.loop(0, 3 * NCH)
    def _(t):
        k = 3 - t // NCH
        i = t % NCH
        jp = (i + 2) % NCH
        jn = i
        ready = (k < 3) | (i >= 2)

        @pl.when(ready)
        def _():
            wait_bytes(rp_b.at[k, jp], rs_recv.at[0, k, jp])
            wait_bytes(rn_b.at[k, jn], rs_recv.at[1, k, jn])
            sp_b[k - 1, jp] = (zs[4 + k, jp] + rp_b[k, jp].astype(F32)).astype(BF16)
            sn_b[k - 1, jn] = (zs[k, jn] + rn_b[k, jn].astype(F32)).astype(BF16)

        @pl.when(jnp.logical_not(ready))
        def _():
            sp_b[k - 1, jp] = zs[4 + k, jp].astype(BF16)
            sn_b[k - 1, jn] = zs[k, jn].astype(BF16)

        rcopy(
            sp_b.at[k - 1, jp], rp_b.at[k - 1, jp], rs_send.at[0, k - 1], rs_recv.at[0, k - 1, jp], r_dev
        ).start()
        rcopy(
            sn_b.at[k - 1, jn], rn_b.at[k - 1, jn], rs_send.at[1, k - 1], rs_recv.at[1, k - 1, jn], l_dev
        ).start()

    for j in range(NCH):
        wait_bytes(rp_b.at[0, j], rs_recv.at[0, 0, j])
        wait_bytes(rn_b.at[0, j], rs_recv.at[1, 0, j])
        total = zs[0, j] + rp_b[0, j].astype(F32) + rn_b[0, j].astype(F32)
        for s in range(2):
            for n in range(width // 128):
                lanes = slice(n * 128, (n + 1) * 128)
                rowsf[n, pl.ds(2 * j + s, nsp, stride=8), :] = total[s * nsp : (s + 1) * nsp, lanes]
    done = jnp.concatenate([rowsf[n] for n in range(width // 128)], axis=1)
    bm[...] = done.reshape(nsp, 8, width).astype(BF16)

    @pl.loop(1, nsp)
    def _(i):
        dst = (me + i) % nsp
        rcopy(bm.at[dst], br.at[me], bsem.at[0], bsem.at[1], {"sp": dst}).start()

    br[me] = bm[me]
    wait_bytes(br.at[pl.ds(0, others)], bsem.at[1])
    back = br[...].astype(F32).reshape(nsp * 8, width).astype(BF16)
    mixed = dot(mix_hi, back) + dot(mix_lo, back)
    for j in range(NCH):
        cols = slice(j * width, (j + 1) * width)
        out[:, cols] = (middle[:, cols] + mixed[j * own : (j + 1) * own]).astype(BF16)

    wait_bytes(hl, hsem.at[0])
    wait_bytes(hr, hsem.at[2])
    wait_bytes(tot_r.at[pl.ds(0, others)], tsem.at[0])
    wait_bytes(st_r.at[pl.ds(0, others)], ssem.at[0])
    wait_bytes(sc_r.at[pl.ds(0, others)], osem.at[0])
    wait_bytes(wc.at[:, pl.ds(0, 128 * (ny - 1))], wsem.at[0])
    wait_bytes(mo.at[pl.ds(0, ntp - 1)], psem.at[0])
    wait_bytes(dr.at[pl.ds(0, others)], dsem.at[0])
    wait_bytes(br.at[pl.ds(0, others)], bsem.at[0])
    for way in range(2):
        for k in range(3):
            wait_bytes(xs.at[0], ag_send.at[way, k])
            wait_bytes(xs.at[0], rs_send.at[way, k])
        wait_bytes(xs.at[0, pl.ds(0, 2)], ag_send.at[way, 3])
        wait_bytes(xs.at[0, pl.ds(0, 2)], rs_send.at[way, 3])


def layer(nsp, ntp, resid, v, k, q, og, raw, hdl, extra, vf, kf, qf, gain, wout, ngain, routes, cw, wg, wu, wd):
    ny = ntp // 2
    tokens = v.shape[0]
    own = tokens // ntp
    width = resid.shape[1] // NCH
    ff = wg.shape[2]
    chan = wout.shape[0] // ny
    rows1 = 2 * nsp

    def lanes(x):
        return jnp.pad(x, ((0, 0), (0, 128 - x.shape[1])))

    raw8 = lanes(jnp.concatenate([raw[0], raw[1]], axis=1).astype(F32))
    extra8 = lanes(jnp.concatenate([extra, extra], axis=1))
    rate8 = lanes(-jnp.exp(hdl).reshape(1, 8))
    dma = pltpu.SemaphoreType.DMA
    vmem = pl.BlockSpec(memory_space=pltpu.VMEM)
    hbm = pl.BlockSpec(memory_space=pl.ANY)
    pair = (nsp, 16, 128)
    msg = (nsp, 8, width)
    ring = (4, NCH, rows1, width)
    scratch = [
        pltpu.VMEM((16, 512), BF16),
        pltpu.VMEM((16, 512), BF16),
        pltpu.VMEM((tokens + 32, 512), F32),
        pltpu.VMEM((8, 128), F32),
        pltpu.VMEM((nsp, 8, 128), F32),
        pltpu.VMEM(pair, BF16),
        pltpu.VMEM(pair, BF16),
        pltpu.VMEM(pair, F32),
        pltpu.VMEM(pair, BF16),
        pltpu.VMEM(pair, BF16),
        pltpu.VMEM((2, tokens, 256), BF16),
        pltpu.VMEM((chan, 128 * ny), BF16),
        pltpu.VMEM((ntp, own, 128 * ny), BF16),
        pltpu.VMEM((ntp, own, 128 * ny), BF16),
        pltpu.VMEM(msg, BF16),
        pltpu.VMEM(msg, BF16),
        pltpu.VMEM((width // 128, nsp * 8, 128), F32),
        pltpu.VMEM((8, NCH, rows1, width), BF16),
        pltpu.VMEM((wg.shape[1], 4 * ff), BF16),
        pltpu.VMEM((2 * ff, wd.shape[2]), BF16),
        pltpu.VMEM((2 * rows1, 4 * ff), F32),
        pltpu.VMEM((8, NCH, rows1, width), F32),
        pltpu.VMEM(ring, BF16),
        pltpu.VMEM(ring, BF16),
        pltpu.VMEM(ring, BF16),
        pltpu.VMEM(ring, BF16),
        pltpu.VMEM(msg, BF16),
        pltpu.VMEM(msg, BF16),
        dma((4,)),
        dma((4,)),
        dma((2,)),
        dma((2,)),
        dma((2,)),
        dma((2,)),
        dma((2,)),
        dma((6,)),
        dma((2,)),
        dma((2,)),
        dma((2, 4)),
        dma((2, 5, NCH)),
        dma((2, 4)),
        dma((2, 4, NCH)),
        dma((2,)),
    ]
    return pl.pallas_call(
        functools.partial(body, nsp, ntp),
        out_shape=jax.ShapeDtypeStruct(resid.shape, BF16),
        in_specs=[vmem] * 12 + [hbm] + [vmem] * 3 + [hbm] * 3,
        out_specs=vmem,
        scratch_shapes=scratch,
        compiler_params=pltpu.CompilerParams(
            collective_id=0, has_side_effects=True, vmem_limit_bytes=56 * 1024 * 1024
        ),
        name="layer",
    )(
        resid,
        v,
        k,
        q,
        og,
        raw8,
        extra8,
        rate8,
        vf,
        kf,
        qf,
        gain.reshape(1, -1),
        wout,
        ngain.reshape(1, -1),
        routes,
        cw,
        wg[0],
        wu[0],
        wd[0],
    )


def solution(mesh):
    both = ("sp", "tp")
    return jax.shard_map(
        functools.partial(layer, mesh.shape["sp"], mesh.shape["tp"]),
        mesh=mesh,
        in_specs=(
            P(both, None),
            P("sp", "tp"),
            P("sp", "tp"),
            P("sp", "tp"),
            P("sp", "tp"),
            P(None, "sp", "tp"),
            P(None, "tp"),
            P("sp", "tp"),
            P(None, "tp"),
            P(None, "tp"),
            P(None, "tp"),
            P("tp"),
            P(None, "tp"),
            P(),
            P("sp", None),
            P(both, None),
            P("sp", None, "tp"),
            P("sp", None, "tp"),
            P("sp", "tp", None),
        ),
        out_specs=P(both, None),
        check_vma=False,
    )
```

time: 413 us -> 128 us (0.31)
  waiting for transfers between devices: 159 us -> 0 us
  blocking collectives: 144 us -> 0 us
  Pallas kernels: 0 us -> 119 us
  local copies, waits for them, and re-layouts: 35.1 us -> 6.56 us
  matrix products: 23.8 us -> 0 us
  starting transfers between devices: 21.2 us -> 0 us
  between operations: 14.4 us -> 0.05 us
  other arithmetic: 13.4 us -> 0.68 us
    pallas_call x0 -> x1, Pallas kernels: none -> 119 us  [layer(): pl.pallas_call(functools.partial(body, nsp, ntp), out_shape=jax.ShapeDtyp...]
    all_gather x7 -> x0, blocking collectives: 112 us -> none  [the longest x6 110 us: carried_in(): lax.all_gather(part.astype(kind), axis)]
    all_gather x2 -> x0, waiting for transfers between devices: 76.8 us -> none  [the longest x1 40.7 us: gather_axes(): filled = lax.all_gather(filled, axes[number], axis=dim, tiled=True)]
    reduce_scatter x1 -> x0, waiting for transfers between devices: 64.6 us -> none  [shards(): lax.psum_scatter(partial_sum.astype(jnp.float32).reshape(arrived.shape).a...]
    dot_general x13 -> x0, matrix products: 23.8 us -> none  [the longest x1 9.1 us: shards(): jnp.dot(hidden, expert_down_matrix[0], preferred_element_type=jnp.float32)]
    all_to_all x1 -> x0, blocking collectives: 22.2 us -> none  [shards(): lax.all_to_all(outgoing.reshape(experts, capacity, model_width), SP, spli...]
    all_to_all x2 -> x0, waiting for transfers between devices: 17.4 us -> none  [the longest x1 9.83 us: shards(): lax.all_to_all(results, SP, split_axis=0, concat_axis=0, tiled=True)]
    all_to_all x2 -> x0, starting transfers between devices: 14.8 us -> none  [the longest x1 10.5 us: shards(): lax.all_to_all(results, SP, split_axis=0, concat_axis=0, tiled=True)]
  transfers between devices with their start and end apart: 7 -> 0, of which waited for: 5 -> 0; matrix products, arithmetic and copies ran while one was open for 3% -> 0% of each run, Pallas kernels for 0% -> 0%
where the time goes in v1:
time: 128 us; the launch traced here: 127 us
  Pallas kernels  119 us (93%)
  local copies, waits for them, and re-layouts  6.56 us (5%)
    pallas_call x1, Pallas kernels, layer(): pl.pallas_call(functools.partial(body, nsp, ntp), out_shape=jax.ShapeDtyp...  119 us
    unnamed x13, local copies, waits for them, and re-layouts  4.97 us

profile of v1, /device:TPU:6, one launch (start us, length us, event | category | flops | bytes accessed | tf_op | source)
XLA Modules:
  0.0 126.6 jit_solution(13827683135032705111)
XLA Ops:
  0.0 0.0 copy-start.4
  0.0 0.0 copy-start.1
  0.0 0.7 copy-done.4
  0.7 0.1 neg.15
  0.8 0.6 pad.16.rate_in
  1.4 0.0 copy-done.1
  1.4 0.0 copy-start
  1.4 0.7 copy-done
  2.1 0.0 copy-start.3
  2.1 0.7 copy-done.3
  2.7 0.7 copy.29.cw_in
  3.4 0.1 copy.26
  3.5 0.7 pad_convert_fusion.raw_in
  4.2 0.1 copy.27
  4.3 0.0 copy-start.2
  4.3 0.7 pad.15.extra_in
  5.0 0.0 copy-done.2
  5.0 0.8 copy.28.routes_in
  5.8 119.4 %layer.1 = bf16[16,2048]{1,0:T(8,128)(2,1)} custom-call(bf16[16,2048]{1,0:T(8,128)(2,1)} %resid.1, bf16[256,256]{1,0:T(8,128)(2,1)} %v_in.1, bf16[256,128]{1,0:T(8,128)(2,1)} %k_in.1, bf16[256,128]{1,0:T(8,128)(2,1)} %q_in.1, bf16[256,256]{1,0:T(8,128)(2,1)} %og_in.1, f32[256,128]{1,0:T(8,128)} %pad_convert_fusion.raw_in, f32[256,128]{1,0:T(8,128)} %pad.15.extra_in, ...), custom_call_target="tpu_custom_call" | custom-call | tf_op jit(solution)/shard_map/layer/pallas_call | solution.py:603
  125.2 1.5 %copy.31 = bf16[16,2048]{1,0:T(8,128)(2,1)} copy(bf16[16,2048]{1,0:T(8,128)(2,1)} %layer.1) | data formatting | bytes 131072
  (4 shorter events, 0.0 us)
Async XLA Ops:
  0.0 0.7 copy-start.4
  0.0 1.4 %copy-start.1 = (bf16[2,256,4]{1,2,0:T(4,128)(2,1)S(1)}, bf16[2,256,4]{1,2,0:T(4,128)(2,1)}, u32[]{:S(2)}) copy-start(bf16[2,256,4]{1,2,0:T(4,128)(2,1)} %param.24) | copy-start | bytes 12292
  1.4 0.7 copy-start
  2.1 0.7 copy-start.3
  4.3 0.7 copy-start.2

commit v2 on v1

--- a/solution.py
+++ b/solution.py
@@ -14,6 +14,8 @@
 EPS = 1e-06
 BLOCK = 128
 NCH = 4
+WIDE = 1024
+NSMALL = 15
 
 
 def dot(a, b, contract=((1,), (0,)), precision=None):
@@ -36,6 +38,11 @@
     pltpu.make_async_copy(ref, ref, sem).wait()
 
 
+def peer(i, me, n):
+    step = n - 2 - i
+    return (me + jnp.where(step % 2 == 0, step // 2 + 1, n - 1 - step // 2)) % n
+
+
 def iota(shape, dim):
     return lax.broadcasted_iota(jnp.int32, shape, dim)
 
@@ -43,26 +50,14 @@
 def body(
     nsp,
     ntp,
-    resid,
-    v_in,
-    k_in,
-    q_in,
-    og_in,
-    raw_in,
-    extra_in,
-    rate_in,
-    vf_in,
-    kf_in,
-    qf_in,
-    gain_in,
-    wout,
-    ngain_in,
-    routes_in,
-    cw_in,
-    wg,
-    wu,
-    wd,
-    out,
+    *refs,
+):
+    small_hbm, (wout, wg, wu, wd), out = refs[:NSMALL], refs[NSMALL : NSMALL + 4], refs[NSMALL + 4]
+    small = refs[NSMALL + 5 : 2 * NSMALL + 5]
+    resid, v_in, k_in, q_in, og_in, raw_in, hdl_in, extra_in = small[:8]
+    vf_in, kf_in, qf_in, gain_in, ngain_in, routes_in, cw_in = small[8:]
+    (
+    raw8,
     hl,
     hr,
     pad,
@@ -106,7 +101,8 @@
     rs_send,
     rs_recv,
     bsem,
-):
+    isem,
+    ) = refs[2 * NSMALL + 5 :]
     me = lax.axis_index("sp")
     tp = lax.axis_index("tp")
     ny = ntp // 2
@@ -116,6 +112,11 @@
     right_y = ((y + 1) % ny) * 2 + c
     left_y = ((y + ny - 1) % ny) * 2 + c
     others = nsp - 1
+    inputs = [
+        pltpu.make_async_copy(src, dst, isem.at[n]) for n, (src, dst) in enumerate(zip(small_hbm, small))
+    ]
+    for n in (5, 6, 7, 1, 2, 3, 8, 9, 10, 4, 13, 14, 0, 11, 12):
+        inputs[n].start()
 
     bar = pltpu.get_barrier_semaphore()
 
@@ -139,50 +140,65 @@
     for load in loads:
         load.start()
 
+    for n in (5, 6, 7):
+        inputs[n].wait()
+    raw8[0, 0:4] = raw_in[0].astype(F32)
+    raw8[0, 4:8] = raw_in[1].astype(F32)
+    raw8[1, 0:4] = extra_in[...]
+    raw8[1, 4:8] = extra_in[...]
+    sub = iota((8, 1), 0)
+    rates = jnp.where(
+        sub < 4, jnp.broadcast_to(hdl_in[0:1], (8, 4)), jnp.broadcast_to(hdl_in[1:2], (8, 4))
+    )
+    rates = jnp.sum(jnp.where(iota((8, 4), 0) % 4 == iota((8, 4), 1), rates, 0.0), axis=1, keepdims=True)
+    step8 = raw8[0]
+    step8 = jnp.maximum(step8, 0.0) + jnp.log1p(jnp.exp(-jnp.abs(step8)))
+    log8 = raw8[1] - jnp.exp(rates) * step8
     lane = iota((1, 128), 1)
-    step8 = raw_in[...]
-    step8 = jnp.maximum(step8, 0.0) + jnp.log1p(jnp.exp(-jnp.abs(step8)))
-    log8 = rate_in[...] * step8 + extra_in[...]
     row = iota((BLOCK, BLOCK), 0)
     col = iota((BLOCK, BLOCK), 1)
-    lower = (col <= row).astype(F32)
-    ones = jnp.ones((BLOCK, BLOCK), F32)
-    spread = ((iota((128, 512), 1) // 64) == iota((128, 512), 0)).astype(F32)
+    upper = (row <= col).astype(F32)
+    spread = ((iota((8, 512), 1) // 64) == iota((8, 512), 0)).astype(F32)
     cum, cum_t, tot_c, sw8, rd8 = [], [], [], [], []
     for b in range(2):
-        logs = log8[b * BLOCK : (b + 1) * BLOCK]
-        run = dot(lower, logs, precision=HIGH)
-        total = run[BLOCK - 1 : BLOCK]
-        both = run - jnp.where(lane >= 4, logs, 0.0)
-        cum.append(both)
-        cum_t.append(both.T)
-        tot_c.append(dot(logs, ones, ((0,), (0,)), HIGH)[0:8])
-        sw8.append(jnp.exp(jnp.where(lane < 4, total - both, both)))
-        rd8.append(jnp.exp(jnp.where(lane < 4, both, total - both)))
+        logs = log8[:, b * BLOCK : (b + 1) * BLOCK]
+        run = dot(logs, upper, precision=HIGH)
+        total = run[:, BLOCK - 1 : BLOCK]
+        both = jnp.where(sub < 4, run, run - logs)
+        cum_t.append(both)
+        cum.append(jnp.concatenate([both, jnp.zeros((120, BLOCK), F32)], axis=0).T)
+        tot_c.append(jnp.broadcast_to(total, (8, 128)))
+        sw8.append(jnp.exp(jnp.where(sub < 4, total - both, both)))
+        rd8.append(jnp.exp(jnp.where(sub < 4, both, total - both)))
     tot_dev = jnp.exp(tot_c[0] + tot_c[1])
     tot_s[...] = tot_dev
     tot_r[me] = tot_dev
-    step_x = dot(step8, spread, precision=HIGH)
-    sw_x = [dot(sw8[b], spread, precision=HIGH) for b in range(2)]
-    rd_x = [dot(rd8[b], spread, precision=HIGH) for b in range(2)]
+    first = ((0,), (0,))
+    step_x = dot(step8, spread, first, HIGH)
+    sw_x = [dot(sw8[b], spread, first, HIGH) for b in range(2)]
+    rd_x = [dot(rd8[b], spread, first, HIGH) for b in range(2)]
 
     def head_rows(b, first):
         e = jnp.exp(tot_c[b][first : first + 4])
         return jnp.concatenate([jnp.broadcast_to(e[h : h + 1], (64, 128)) for h in range(4)], axis=0)
 
+    tokens = v_in.shape[0]
+    for n in (1, 2, 3):
+        inputs[n].wait()
+    pad[16 : 16 + tokens, 0:256] = v_in[...].astype(F32)
+    pad[16 : 16 + tokens, 256:384] = k_in[...].astype(F32)
+    pad[16 : 16 + tokens, 384:512] = q_in[...].astype(F32)
+    for n in (0, 4, *range(8, NSMALL)):
+        inputs[n].wait()
+
     pl.semaphore_wait(bar, nsp - 1 + ntp - 1)
 
     right = {"sp": (me + 1) % nsp}
     left = {"sp": (me + nsp - 1) % nsp}
-    tokens = v_in.shape[0]
     for ref, lo, width in ((v_in, 0, 256), (k_in, 256, 128), (q_in, 384, 128)):
         cols = pl.ds(lo, width)
         rcopy(ref.at[pl.ds(tokens - 16, 16)], hl.at[:, cols], hsem.at[0], hsem.at[1], right).start()
         rcopy(ref.at[pl.ds(0, 16)], hr.at[:, cols], hsem.at[2], hsem.at[3], left).start()
-
-    @pl.loop(1, nsp)
-    def _(i):
-        rcopy(tot_s, tot_r.at[me], tsem.at[0], tsem.at[1], {"sp": (me + i) % nsp}).start()
 
     @pl.loop(1, ny)
     def _(i):
@@ -195,6 +211,10 @@
             {"tp": dst * 2 + c},
         ).start()
 
+    @pl.loop(0, nsp - 1)
+    def _(i):
+        rcopy(tot_s, tot_r.at[me], tsem.at[0], tsem.at[1], {"sp": peer(i, me, nsp)}).start()
+
     swaps = [
         rcopy(wg, wgu.at[:, pl.ds(ff, ff)], swsem.at[0], swsem.at[1], {"tp": partner}),
         rcopy(wu, wgu.at[:, pl.ds(3 * ff, ff)], swsem.at[2], swsem.at[3], {"tp": partner}),
@@ -203,9 +223,6 @@
     for swap in swaps:
         swap.start()
 
-    pad[16 : 16 + tokens, 0:256] = v_in[...].astype(F32)
-    pad[16 : 16 + tokens, 256:384] = k_in[...].astype(F32)
-    pad[16 : 16 + tokens, 384:512] = q_in[...].astype(F32)
     wait_bytes(hl, hsem.at[1])
     wait_bytes(hr, hsem.at[3])
     pad[0:16] = jnp.where(me > 0, hl[...].astype(F32), 0.0)
@@ -232,9 +249,9 @@
     ).astype(BF16)
     st_s[...] = mine
 
-    @pl.loop(1, nsp)
+    @pl.loop(0, nsp - 1)
     def _(i):
-        dst = (me + i) % nsp
+        dst = peer(i, me, nsp)
         rcopy(st_s.at[dst], st_r.at[me], ssem.at[0], ssem.at[1], {"sp": dst}).start()
 
     st_r[me] = st_s[me]
@@ -263,25 +280,30 @@
         inner.append(jnp.concatenate(pairs, axis=1))
     gate_act = silu(og_in[...].astype(F32))
 
-    own = routes_in.shape[0] // ntp
-    my_routes = routes_in[pl.ds(pl.multiple_of(tp * own, own), own), :]
-    e_lane = iota((own, 128), 1)
-    hot0 = (my_routes[:, 0:1] == e_lane).astype(F32)
-    hot1 = (my_routes[:, 1:2] == e_lane).astype(F32)
+    own = tokens // ntp
+    mine_lane = iota((own, tokens), 1) == iota((own, tokens), 0) + tp * own
+    e_lane = iota((own, 128), 1).astype(F32)
+    hots = []
+    for n in range(2):
+        ids = jnp.where(mine_lane, routes_in[n : n + 1].astype(F32), 0.0)
+        hots.append((jnp.sum(ids, axis=1, keepdims=True) == e_lane).astype(F32))
     strict = (iota((own, own), 1) < iota((own, own), 0)).astype(F32)
-    before = dot(strict, hot0 + hot1, precision=HIGH)
-    ids = e_lane.astype(F32) * 2.0 + before
-    slot0 = jnp.sum(hot0 * ids, axis=1, keepdims=True)
-    slot1 = jnp.sum(hot1 * ids, axis=1, keepdims=True)
-    r_id = iota((NCH * own, nsp * 8), 1)
-    r_slot = ((r_id // 8) * 2 + r_id % 2).astype(F32)
-    same = ((r_id // 2) % 4) == (iota((NCH * own, nsp * 8), 0) // own)
-    hit0 = same & (r_slot == jnp.concatenate([slot0] * NCH, axis=0))
-    hit1 = same & (r_slot == jnp.concatenate([slot1] * NCH, axis=0))
-    place = jnp.where(hit0 | hit1, 1.0, 0.0).astype(BF16)
-    w0 = jnp.concatenate([cw_in[:, 0:1]] * NCH, axis=0)
-    w1 = jnp.concatenate([cw_in[:, 1:2]] * NCH, axis=0)
-    mixing = jnp.where(hit0, w0, 0.0) + jnp.where(hit1, w1, 0.0)
+    ids = e_lane * 2.0 + dot(strict, hots[0] + hots[1], precision=HIGH)
+    tiles = WIDE // 128
+    r_id = iota((tiles * own, nsp * 2 * tiles), 1)
+    t_id = iota((tiles * own, nsp * 2 * tiles), 0)
+    r_slot = ((r_id // (2 * tiles)) * 2 + r_id % 2).astype(F32)
+    same = ((r_id // 2) % tiles) == (t_id // own)
+    w_lane = iota((tiles * own, own), 0) % own == iota((tiles * own, own), 1)
+    mixing = jnp.zeros(r_id.shape, F32)
+    place = jnp.zeros(r_id.shape, F32)
+    for n in range(2):
+        slot = jnp.sum(hots[n] * ids, axis=1, keepdims=True)
+        hit = same & (r_slot == jnp.concatenate([slot] * tiles, axis=0))
+        weight = jnp.sum(jnp.where(w_lane, cw_in[n : n + 1], 0.0), axis=1, keepdims=True)
+        place = jnp.where(hit, 1.0, place)
+        mixing = jnp.where(hit, weight, mixing)
+    place = place.astype(BF16)
     mix_hi = mixing.astype(BF16)
     mix_lo = (mixing - mix_hi.astype(F32)).astype(BF16)
 
@@ -305,9 +327,9 @@
     lax.fori_loop(0, nsp, backward, zero)
     sc_s[...] = sc_f[...].astype(BF16)
 
-    @pl.loop(1, nsp)
+    @pl.loop(0, nsp - 1)
     def _(i):
-        dst = (me + i) % nsp
+        dst = peer(i, me, nsp)
         rcopy(sc_s.at[dst], sc_r.at[me], osem.at[0], osem.at[1], {"sp": dst}).start()
 
     sc_r[me] = sc_s[me]
@@ -360,30 +382,43 @@
     middle = (resid[...].astype(F32) + mixer_out).astype(BF16).astype(F32)
     square = jnp.mean(middle * middle, axis=-1, keepdims=True)
     normed = (middle * lax.rsqrt(square + EPS) * ngain_in[...]).astype(BF16)
+    parts = normed.shape[1] // WIDE
     width = normed.shape[1] // NCH
-    stacked = jnp.concatenate([normed[:, j * width : (j + 1) * width] for j in range(NCH)], axis=0)
-    sent = dot(place, stacked, ((0,), (0,)))
-    dm[...] = sent.reshape(nsp, 8, width).astype(BF16)
-
-    @pl.loop(1, nsp)
-    def _(i):
-        dst = (me + i) % nsp
-        rcopy(dm.at[dst], dr.at[me], dsem.at[0], dsem.at[1], {"sp": dst}).start()
-
-    dr[me] = dm[me]
-    wait_bytes(dr.at[pl.ds(0, others)], dsem.at[1])
-    arrived = dr[...].astype(F32).reshape(nsp * 8, width)
-    for n in range(width // 128):
-        rowsf[n] = arrived[:, n * 128 : (n + 1) * 128]
+    per = NCH // parts
+    stacked = jnp.concatenate(
+        [
+            jnp.concatenate(
+                [normed[:, p * WIDE + n * 128 : p * WIDE + (n + 1) * 128] for n in range(tiles)], axis=0
+            )
+            for p in range(parts)
+        ],
+        axis=1,
+    )
+    sent = dot(place, stacked, first)
+    for p in range(parts):
+        dm[p] = sent[:, p * 128 : (p + 1) * 128].reshape(nsp, 2 * tiles, 128).astype(BF16)
+
+        @pl.loop(0, nsp - 1)
+        def _(i):
+            dst = peer(i, me, nsp)
+            rcopy(dm.at[p, dst], dr.at[p, me], dsem.at[0, p], dsem.at[1, p], {"sp": dst}).start()
+
+        dr[p, me] = dm[p, me]
+
     r_dev = {"tp": right_y}
     l_dev = {"tp": left_y}
-    for j in range(NCH):
-        for s in range(2):
+    for p in range(parts):
+        wait_bytes(dr.at[p, pl.ds(0, others)], dsem.at[1, p])
+        rowsf[...] = dr[p].astype(F32).reshape(nsp * 2 * tiles, 128)
+        for q in range(per):
+            j = p * per + q
             for n in range(width // 128):
-                picked = rowsf[n, pl.ds(2 * j + s, nsp, stride=8), :]
-                xs[0, j, s * nsp : (s + 1) * nsp, n * 128 : (n + 1) * 128] = picked.astype(BF16)
-        rcopy(xs.at[0, j], xs.at[1, j], ag_send.at[0, 0], ag_recv.at[0, 1, j], r_dev).start()
-        rcopy(xs.at[0, j], xs.at[5, j], ag_send.at[1, 0], ag_recv.at[1, 1, j], l_dev).start()
+                for s in range(2):
+                    tile = q * (width // 128) + n
+                    picked = rowsf[pl.ds(2 * tile + s, nsp, stride=2 * tiles), :]
+                    xs[0, j, s * nsp : (s + 1) * nsp, n * 128 : (n + 1) * 128] = picked.astype(BF16)
+            rcopy(xs.at[0, j], xs.at[1, j], ag_send.at[0, 0], ag_recv.at[0, 1, j], r_dev).start()
+            rcopy(xs.at[0, j], xs.at[5, j], ag_send.at[1, 0], ag_recv.at[1, 1, j], l_dev).start()
 
     for load in loads[1:]:
         load.wait()
@@ -391,6 +426,8 @@
         swap.wait()
 
     rows1 = 2 * nsp
+    top = pl.ds(0, nsp)
+    low = pl.ds(nsp, nsp)
 
     def add_chunk(x, j, first):
         n = x.shape[0]
@@ -433,13 +470,14 @@
             rcopy(xs.at[k, j], xs.at[k + 1, j], ag_send.at[0, k], ag_recv.at[0, k + 1, j], r_dev).start()
             rcopy(xs.at[4 + k, j], xs.at[5 + k, j], ag_send.at[1, k], ag_recv.at[1, k + 1, j], l_dev).start()
 
-        @pl.when((k == 3) & (j < 2))
+        @pl.when(k == 3)
         def _():
-            rcopy(xs.at[3, j], xs.at[4, j], ag_send.at[0, 3], ag_recv.at[0, 4, j], r_dev).start()
-
-        @pl.when((k == 3) & (j >= 2))
-        def _():
-            rcopy(xs.at[7, j], xs.at[4, j], ag_send.at[1, 3], ag_recv.at[1, 4, j], l_dev).start()
+            rcopy(
+                xs.at[3, j, top], xs.at[4, j, top], ag_send.at[0, 3], ag_recv.at[0, 4, j], r_dev
+            ).start()
+            rcopy(
+                xs.at[7, j, low], xs.at[4, j, low], ag_send.at[1, 3], ag_recv.at[1, 4, j], l_dev
+            ).start()
 
         add_chunk(jnp.concatenate([xs[k, j], xs[4 + k, j]], axis=0), j, j == 0)
 
@@ -451,71 +489,82 @@
 
             finish(2 * rows1, store)
 
-    for j in (0, 2, 1, 3):
-        wait_bytes(xs.at[4, j], ag_recv.at[0 if j < 2 else 1, 4, j])
+    @pl.loop(0, NCH)
+    def _(j):
+        wait_bytes(xs.at[4, j, top], ag_recv.at[0, 4, j])
+        wait_bytes(xs.at[4, j, low], ag_recv.at[1, 4, j])
         add_chunk(xs[4, j], j, j == 0)
 
     def store_far(j, z):
-        zs[4, j] = z
-        if j < 2:
-            sp_b[3, j] = z.astype(BF16)
-            rcopy(sp_b.at[3, j], rp_b.at[3, j], rs_send.at[0, 3], rs_recv.at[0, 3, j], r_dev).start()
-        else:
-            sn_b[3, j] = z.astype(BF16)
-            rcopy(sn_b.at[3, j], rn_b.at[3, j], rs_send.at[1, 3], rs_recv.at[1, 3, j], l_dev).start()
+        sp_b[3, j, 0:nsp] = z[0:nsp].astype(BF16)
+        sn_b[3, j, nsp:rows1] = z[nsp:rows1].astype(BF16)
+        rcopy(
+            sp_b.at[3, j, top], rp_b.at[3, j, top], rs_send.at[0, 3], rs_recv.at[0, 3, j], r_dev
+        ).start()
+        rcopy(
+            sn_b.at[3, j, low], rn_b.at[3, j, low], rs_send.at[1, 3], rs_recv.at[1, 3, j], l_dev
+        ).start()
 
     finish(rows1, store_far)
 
     @pl.loop(0, 3 * NCH)
     def _(t):
         k = 3 - t // NCH
-        i = t % NCH
-        jp = (i + 2) % NCH
-        jn = i
-        ready = (k < 3) | (i >= 2)
-
-        @pl.when(ready)
+        j = t % NCH
+
+        @pl.when(k == 3)
         def _():
-            wait_bytes(rp_b.at[k, jp], rs_recv.at[0, k, jp])
-            wait_bytes(rn_b.at[k, jn], rs_recv.at[1, k, jn])
-            sp_b[k - 1, jp] = (zs[4 + k, jp] + rp_b[k, jp].astype(F32)).astype(BF16)
-            sn_b[k - 1, jn] = (zs[k, jn] + rn_b[k, jn].astype(F32)).astype(BF16)
-
-        @pl.when(jnp.logical_not(ready))
+            wait_bytes(rp_b.at[3, j, top], rs_recv.at[0, 3, j])
+            wait_bytes(rn_b.at[3, j, low], rs_recv.at[1, 3, j])
+            sp_b[2, j, 0:nsp] = (zs[7, j, 0:nsp] + rp_b[3, j, 0:nsp].astype(F32)).astype(BF16)
+            sp_b[2, j, nsp:rows1] = zs[7, j, nsp:rows1].astype(BF16)
+            sn_b[2, j, 0:nsp] = zs[3, j, 0:nsp].astype(BF16)
+            sn_b[2, j, nsp:rows1] = (
+                zs[3, j, nsp:rows1] + rn_b[3, j, nsp:rows1].astype(F32)
+            ).astype(BF16)
+
+        @pl.when(k < 3)
         def _():
-            sp_b[k - 1, jp] = zs[4 + k, jp].astype(BF16)
-            sn_b[k - 1, jn] = zs[k, jn].astype(BF16)
+            wait_bytes(rp_b.at[k, j], rs_recv.at[0, k, j])
+            wait_bytes(rn_b.at[k, j], rs_recv.at[1, k, j])
+            sp_b[k - 1, j] = (zs[4 + k, j] + rp_b[k, j].astype(F32)).astype(BF16)
+            sn_b[k - 1, j] = (zs[k, j] + rn_b[k, j].astype(F32)).astype(BF16)
 
         rcopy(
-            sp_b.at[k - 1, jp], rp_b.at[k - 1, jp], rs_send.at[0, k - 1], rs_recv.at[0, k - 1, jp], r_dev
+            sp_b.at[k - 1, j], rp_b.at[k - 1, j], rs_send.at[0, k - 1], rs_recv.at[0, k - 1, j], r_dev
         ).start()
         rcopy(
-            sn_b.at[k - 1, jn], rn_b.at[k - 1, jn], rs_send.at[1, k - 1], rs_recv.at[1, k - 1, jn], l_dev
+            sn_b.at[k - 1, j], rn_b.at[k - 1, j], rs_send.at[1, k - 1], rs_recv.at[1, k - 1, j], l_dev
         ).start()
 
-    for j in range(NCH):
-        wait_bytes(rp_b.at[0, j], rs_recv.at[0, 0, j])
-        wait_bytes(rn_b.at[0, j], rs_recv.at[1, 0, j])
-        total = zs[0, j] + rp_b[0, j].astype(F32) + rn_b[0, j].astype(F32)
-        for s in range(2):
+    for p in range(parts):
+        for q in range(per):
+            j = p * per + q
+            wait_bytes(rp_b.at[0, j], rs_recv.at[0, 0, j])
+            wait_bytes(rn_b.at[0, j], rs_recv.at[1, 0, j])
+            total = zs[0, j] + rp_b[0, j].astype(F32) + rn_b[0, j].astype(F32)
             for n in range(width // 128):
-                lanes = slice(n * 128, (n + 1) * 128)
-                rowsf[n, pl.ds(2 * j + s, nsp, stride=8), :] = total[s * nsp : (s + 1) * nsp, lanes]
-    done = jnp.concatenate([rowsf[n] for n in range(width // 128)], axis=1)
-    bm[...] = done.reshape(nsp, 8, width).astype(BF16)
-
-    @pl.loop(1, nsp)
-    def _(i):
-        dst = (me + i) % nsp
-        rcopy(bm.at[dst], br.at[me], bsem.at[0], bsem.at[1], {"sp": dst}).start()
-
-    br[me] = bm[me]
-    wait_bytes(br.at[pl.ds(0, others)], bsem.at[1])
-    back = br[...].astype(F32).reshape(nsp * 8, width).astype(BF16)
-    mixed = dot(mix_hi, back) + dot(mix_lo, back)
-    for j in range(NCH):
-        cols = slice(j * width, (j + 1) * width)
-        out[:, cols] = (middle[:, cols] + mixed[j * own : (j + 1) * own]).astype(BF16)
+                for s in range(2):
+                    tile = q * (width // 128) + n
+                    rowsf[pl.ds(2 * tile + s, nsp, stride=2 * tiles), :] = total[
+                        s * nsp : (s + 1) * nsp, n * 128 : (n + 1) * 128
+                    ]
+        bm[p] = rowsf[...].reshape(nsp, 2 * tiles, 128).astype(BF16)
+
+        @pl.loop(0, nsp - 1)
+        def _(i):
+            dst = peer(i, me, nsp)
+            rcopy(bm.at[p, dst], br.at[p, me], bsem.at[0, p], bsem.at[1, p], {"sp": dst}).start()
+
+        br[p, me] = bm[p, me]
+
+    for p in range(parts):
+        wait_bytes(br.at[p, pl.ds(0, others)], bsem.at[1, p])
+        back = br[p].astype(F32).reshape(nsp * 2 * tiles, 128).astype(BF16)
+        mixed = dot(mix_hi, back) + dot(mix_lo, back)
+        for n in range(tiles):
+            cols = slice(p * WIDE + n * 128, p * WIDE + (n + 1) * 128)
+            out[:, cols] = (middle[:, cols] + mixed[n * own : (n + 1) * own]).astype(BF16)
 
     wait_bytes(hl, hsem.at[0])
     wait_bytes(hr, hsem.at[2])
@@ -524,8 +573,9 @@
     wait_bytes(sc_r.at[pl.ds(0, others)], osem.at[0])
     wait_bytes(wc.at[:, pl.ds(0, 128 * (ny - 1))], wsem.at[0])
     wait_bytes(mo.at[pl.ds(0, ntp - 1)], psem.at[0])
-    wait_bytes(dr.at[pl.ds(0, others)], dsem.at[0])
-    wait_bytes(br.at[pl.ds(0, others)], bsem.at[0])
+    for p in range(parts):
+        wait_bytes(dr.at[p, pl.ds(0, others)], dsem.at[0, p])
+        wait_bytes(br.at[p, pl.ds(0, others)], bsem.at[0, p])
     for way in range(2):
         for k in range(3):
             wait_bytes(xs.at[0], ag_send.at[way, k])
@@ -543,19 +593,31 @@
     chan = wout.shape[0] // ny
     rows1 = 2 * nsp
 
-    def lanes(x):
-        return jnp.pad(x, ((0, 0), (0, 128 - x.shape[1])))
-
-    raw8 = lanes(jnp.concatenate([raw[0], raw[1]], axis=1).astype(F32))
-    extra8 = lanes(jnp.concatenate([extra, extra], axis=1))
-    rate8 = lanes(-jnp.exp(hdl).reshape(1, 8))
+    small = [
+        resid,
+        v,
+        k,
+        q,
+        og,
+        raw.transpose(0, 2, 1),
+        hdl,
+        extra.T,
+        vf,
+        kf,
+        qf,
+        gain.reshape(1, -1),
+        ngain.reshape(1, -1),
+        routes.T,
+        cw.T,
+    ]
     dma = pltpu.SemaphoreType.DMA
-    vmem = pl.BlockSpec(memory_space=pltpu.VMEM)
     hbm = pl.BlockSpec(memory_space=pl.ANY)
     pair = (nsp, 16, 128)
-    msg = (nsp, 8, width)
+    parts = resid.shape[1] // WIDE
+    msg = (parts, nsp, WIDE // 64, 128)
     ring = (4, NCH, rows1, width)
-    scratch = [
+    scratch = [pltpu.VMEM(x.shape, x.dtype) for x in small] + [
+        pltpu.VMEM((2, 8, tokens), F32),
         pltpu.VMEM((16, 512), BF16),
         pltpu.VMEM((16, 512), BF16),
         pltpu.VMEM((tokens + 32, 512), F32),
@@ -572,7 +634,7 @@
         pltpu.VMEM((ntp, own, 128 * ny), BF16),
         pltpu.VMEM(msg, BF16),
         pltpu.VMEM(msg, BF16),
-        pltpu.VMEM((width // 128, nsp * 8, 128), F32),
+        pltpu.VMEM((nsp * WIDE // 64, 128), F32),
         pltpu.VMEM((8, NCH, rows1, width), BF16),
         pltpu.VMEM((wg.shape[1], 4 * ff), BF16),
         pltpu.VMEM((2 * ff, wd.shape[2]), BF16),
@@ -593,44 +655,25 @@
         dma((2,)),
         dma((6,)),
         dma((2,)),
-        dma((2,)),
+        dma((2, parts)),
         dma((2, 4)),
         dma((2, 5, NCH)),
         dma((2, 4)),
         dma((2, 4, NCH)),
-        dma((2,)),
+        dma((2, parts)),
+        dma((NSMALL,)),
     ]
     return pl.pallas_call(
         functools.partial(body, nsp, ntp),
         out_shape=jax.ShapeDtypeStruct(resid.shape, BF16),
-        in_specs=[vmem] * 12 + [hbm] + [vmem] * 3 + [hbm] * 3,
-        out_specs=vmem,
+        in_specs=[hbm] * (NSMALL + 4),
+        out_specs=pl.BlockSpec(memory_space=pltpu.VMEM),
         scratch_shapes=scratch,
         compiler_params=pltpu.CompilerParams(
             collective_id=0, has_side_effects=True, vmem_limit_bytes=56 * 1024 * 1024
         ),
         name="layer",
-    )(
-        resid,
-        v,
-        k,
-        q,
-        og,
-        raw8,
-        extra8,
-        rate8,
-        vf,
-        kf,
-        qf,
-        gain.reshape(1, -1),
-        wout,
-        ngain.reshape(1, -1),
-        routes,
-        cw,
-        wg[0],
-        wu[0],
-        wd[0],
-    )
+    )(*small, wout, wg[0], wu[0], wd[0])
 
 
 def solution(mesh):

time: 128 us -> 118 us (0.922)
  local copies, waits for them, and re-layouts: 6.56 us -> 1.47 us
  Pallas kernels: 119 us -> 115 us
    pallas_call x1, Pallas kernels: 119 us -> 115 us  [layer(): pl.pallas_call(functools.partial(body, nsp, ntp), out_shape=jax.ShapeDtyp...]
    unnamed x13 -> x1, local copies, waits for them, and re-layouts: 4.97 us -> 1.47 us
where the time goes in v2:
time: 118 us; the launch traced here: 117 us
  Pallas kernels  115 us (97%)
  local copies, waits for them, and re-layouts  1.47 us (1%)
    pallas_call x1, Pallas kernels, layer(): pl.pallas_call(functools.partial(body, nsp, ntp), out_shape=jax.ShapeDtyp...  115 us

profile of v2, /device:TPU:6, one launch (start us, length us, event | category | flops | bytes accessed | tf_op | source)
XLA Modules:
  0.0 117.0 jit_solution(4125304906401492031)
XLA Ops:
  0.0 115.5 %layer.1 = bf16[16,2048]{1,0:T(8,128)(2,1)} custom-call(bf16[16,2048]{1,0:T(8,128)(2,1)} %refs_0_.1, bf16[256,256]{1,0:T(8,128)(2,1)} %refs_1_.1, bf16[256,128]{1,0:T(8,128)(2,1)} %refs_2_.1, bf16[256,128]{1,0:T(8,128)(2,1)} %refs_3_.1, bf16[256,256]{1,0:T(8,128)(2,1)} %refs_4_.1, bf16[2,4,256]{2,1,0:T(4,128)(2,1)} %bitcast.13, f32[2,4]{1,0:T(2,128)} %refs_6_.1, ...), custom_call_target="tpu_custom_call" | custom-call | tf_op jit(solution)/shard_map/layer/pallas_call | solution.py:666
  115.5 1.5 %copy.21 = bf16[16,2048]{1,0:T(8,128)(2,1)} copy(bf16[16,2048]{1,0:T(8,128)(2,1)} %layer.1) | data formatting | bytes 131072

commit v3 on v2

--- a/solution.py
+++ b/solution.py
@@ -14,7 +14,8 @@
 EPS = 1e-06
 BLOCK = 128
 NCH = 4
-WIDE = 1024
+NX = 4
+WIDE = 512
 NSMALL = 15
 
 
@@ -63,6 +64,7 @@
     pad,
     tot_s,
     tot_r,
+    decay,
     st_s,
     st_r,
     sc_f,
@@ -72,6 +74,8 @@
     wc,
     po,
     mo,
+    near,
+    through,
     dm,
     dr,
     rowsf,
@@ -79,6 +83,7 @@
     wgu,
     wdn,
     acc,
+    hidden,
     zs,
     sp_b,
     sn_b,
@@ -93,8 +98,11 @@
     osem,
     hdsem,
     wsem,
+    wsend,
+    wrecv,
     swsem,
     psem,
+    nsem,
     dsem,
     ag_send,
     ag_recv,
@@ -130,12 +138,24 @@
 
     ff = wg.shape[1]
     chan = wout.shape[0] // ny
-    ycol = pl.ds(pl.multiple_of(y * 128, 128), 128)
+    nx = NX
+    x = me % nx
+    turns = ny // nx
+
+    def w_rows(of):
+        return wout.at[pl.ds(pl.multiple_of(of * chan, chan), chan)]
+
+    def w_block(of):
+        return wc.at[:, pl.ds(pl.multiple_of(of * 128, 128), 128)]
+
+    @pl.when(x == 0)
+    def _():
+        pltpu.make_async_copy(w_rows(y), w_block(y), wrecv.at[0]).start()
+
     loads = [
-        pltpu.make_async_copy(wout.at[pl.ds(pl.multiple_of(y * chan, chan), chan)], wc.at[:, ycol], lsem.at[0]),
-        pltpu.make_async_copy(wg, wgu.at[:, pl.ds(0, ff)], lsem.at[1]),
-        pltpu.make_async_copy(wu, wgu.at[:, pl.ds(2 * ff, ff)], lsem.at[2]),
-        pltpu.make_async_copy(wd, wdn.at[pl.ds(0, ff)], lsem.at[3]),
+        pltpu.make_async_copy(wg, wgu.at[:, pl.ds(0, ff)], lsem.at[0]),
+        pltpu.make_async_copy(wu, wgu.at[:, pl.ds(2 * ff, ff)], lsem.at[1]),
+        pltpu.make_async_copy(wd, wdn.at[pl.ds(0, ff)], lsem.at[2]),
     ]
     for load in loads:
         load.start()
@@ -171,8 +191,9 @@
         sw8.append(jnp.exp(jnp.where(sub < 4, total - both, both)))
         rd8.append(jnp.exp(jnp.where(sub < 4, both, total - both)))
     tot_dev = jnp.exp(tot_c[0] + tot_c[1])
-    tot_s[...] = tot_dev
-    tot_r[me] = tot_dev
+    tot_row = jnp.sum(jnp.where(sub == lane, tot_dev, 0.0), axis=0, keepdims=True)
+    tot_s[...] = tot_row
+    tot_r[me] = tot_row
     first = ((0,), (0,))
     step_x = dot(step8, spread, first, HIGH)
     sw_x = [dot(sw8[b], spread, first, HIGH) for b in range(2)]
@@ -200,28 +221,27 @@
         rcopy(ref.at[pl.ds(tokens - 16, 16)], hl.at[:, cols], hsem.at[0], hsem.at[1], right).start()
         rcopy(ref.at[pl.ds(0, 16)], hr.at[:, cols], hsem.at[2], hsem.at[3], left).start()
 
-    @pl.loop(1, ny)
-    def _(i):
-        dst = (y + i) % ny
-        rcopy(
-            wout.at[pl.ds(pl.multiple_of(dst * chan, chan), chan)],
-            wc.at[:, ycol],
-            wsem.at[0],
-            wsem.at[1],
-            {"tp": dst * 2 + c},
-        ).start()
-
     @pl.loop(0, nsp - 1)
     def _(i):
         rcopy(tot_s, tot_r.at[me], tsem.at[0], tsem.at[1], {"sp": peer(i, me, nsp)}).start()
 
-    swaps = [
-        rcopy(wg, wgu.at[:, pl.ds(ff, ff)], swsem.at[0], swsem.at[1], {"tp": partner}),
-        rcopy(wu, wgu.at[:, pl.ds(3 * ff, ff)], swsem.at[2], swsem.at[3], {"tp": partner}),
-        rcopy(wd, wdn.at[pl.ds(ff, ff)], swsem.at[4], swsem.at[5], {"tp": partner}),
-    ]
-    for swap in swaps:
-        swap.start()
+    def w_send(m):
+        dst = (y + ny - x - m * nx) % ny
+        return rcopy(w_rows(dst), w_block(y), wsend.at[m], wrecv.at[m], {"tp": dst * 2 + c})
+
+    @pl.when(x > 0)
+    def _():
+        w_send(0).start()
+
+    for m in range(1, turns):
+        w_send(m).start()
+
+    def w_relay(m):
+        block = w_block((y + x + m * nx) % ny)
+        wait_bytes(block, wrecv.at[m])
+        for i in range(1, nx):
+            to = me - x + (x + i) % nx
+            rcopy(block, block, wsem.at[0], wsem.at[1], {"sp": to}).start()
 
     wait_bytes(hl, hsem.at[1])
     wait_bytes(hr, hsem.at[3])
@@ -307,20 +327,24 @@
     mix_hi = mixing.astype(BF16)
     mix_lo = (mixing - mix_hi.astype(F32)).astype(BF16)
 
+    w_relay(0)
+
     wait_bytes(tot_r.at[pl.ds(0, others)], tsem.at[1])
     wait_bytes(st_r.at[pl.ds(0, others)], ssem.at[1])
     head = me // (64 // piece)
+    totals = jnp.concatenate([tot_r[d] for d in range(nsp)], axis=0)
+    for n in range(2):
+        of_head = jnp.sum(jnp.where(lane == head + 4 * n, totals, 0.0), axis=1, keepdims=True)
+        decay[n] = jnp.broadcast_to(of_head, (nsp, 128))
 
     def forward(d, carry):
         sc_f[d, 0:piece] = carry
-        decay = tot_r[d, pl.ds(head, 1), :]
-        return decay * carry + st_r[d].astype(F32)[0:piece]
+        return decay[0, pl.ds(d, 1), :] * carry + st_r[d].astype(F32)[0:piece]
 
     def backward(i, carry):
         d = nsp - 1 - i
         sc_f[d, piece : 2 * piece] = carry
-        decay = tot_r[d, pl.ds(head + 4, 1), :]
-        return decay * carry + st_r[d].astype(F32)[piece : 2 * piece]
+        return decay[1, pl.ds(d, 1), :] * carry + st_r[d].astype(F32)[piece : 2 * piece]
 
     zero = jnp.zeros((piece, 128), F32)
     lax.fori_loop(0, nsp, forward, zero)
@@ -333,6 +357,9 @@
         rcopy(sc_s.at[dst], sc_r.at[me], osem.at[0], osem.at[1], {"sp": dst}).start()
 
     sc_r[me] = sc_s[me]
+    for m in range(1, turns):
+        w_relay(m)
+
     wait_bytes(sc_r.at[pl.ds(0, others)], osem.at[1])
 
     around = sc_r[...].astype(F32)
@@ -353,8 +380,8 @@
     swap_h = rcopy(heads.at[c], heads.at[c], hdsem.at[0], hdsem.at[1], {"tp": partner})
     swap_h.start()
 
-    loads[0].wait()
-    wait_bytes(wc.at[:, pl.ds(0, 128 * (ny - 1))], wsem.at[1])
+    far_w = wc.at[:, pl.ds(0, 128 * (ny - turns))]
+    wait_bytes(far_w, wsem.at[1])
     inner_c = chan // 2
     own_part = dot(heads[c], wc[pl.ds(pl.multiple_of(c * inner_c, inner_c), inner_c), :])
     swap_h.wait()
@@ -362,18 +389,49 @@
     full = own_part + dot(heads[o_c], wc[pl.ds(pl.multiple_of(o_c * inner_c, inner_c), inner_c), :])
     po[...] = full.reshape(ntp, own, full.shape[1]).astype(BF16)
 
-    @pl.loop(1, ntp)
-    def _(i):
-        dst = (tp + i) % ntp
-        rcopy(po.at[dst], mo.at[tp], psem.at[0], psem.at[1], {"tp": dst}).start()
-
+    def chip(distance, core):
+        return ((y + ny + distance) % ny) * 2 + core
+
+    relays = []
+    for way in range(2):
+        sign = 1 - 2 * way
+        for core in range(2):
+            copy = rcopy(
+                po.at[chip(3 * sign, core)],
+                near.at[way, core],
+                nsem.at[0, way, core],
+                nsem.at[1, way, core],
+                {"tp": chip(sign, c)},
+            )
+            copy.start()
+            relays.append(copy)
+    for distance in (4, 1, -1):
+        for core in range(2):
+            dst = chip(distance, core)
+            rcopy(po.at[dst], mo.at[tp], psem.at[0], psem.at[1], {"tp": dst}).start()
+    rcopy(po.at[partner], mo.at[tp], psem.at[0], psem.at[1], {"tp": partner}).start()
     mo[tp] = po[tp]
-    wait_bytes(mo.at[pl.ds(0, ntp - 1)], psem.at[1])
+    for way in range(2):
+        for core in range(2):
+            dst = chip(2 - 4 * way, core)
+            relays[2 * way + core].wait_recv()
+            through[way, core] = (po[dst].astype(F32) + near[way, core].astype(F32)).astype(BF16)
+            rcopy(through.at[way, core], mo.at[tp], psem.at[0], psem.at[1], {"tp": dst}).start()
+
+    swaps = [
+        rcopy(wg, wgu.at[:, pl.ds(ff, ff)], swsem.at[0], swsem.at[1], {"tp": partner}),
+        rcopy(wu, wgu.at[:, pl.ds(3 * ff, ff)], swsem.at[2], swsem.at[3], {"tp": partner}),
+        rcopy(wd, wdn.at[pl.ds(ff, ff)], swsem.at[4], swsem.at[5], {"tp": partner}),
+    ]
+    for swap in swaps:
+        swap.start()
+
+    wait_bytes(mo.at[pl.ds(0, ntp - 5)], psem.at[1])
     halves = []
     for core in range(2):
-        total = mo[core].astype(F32)
-        for other in range(1, ny):
-            total = total + mo[2 * other + core].astype(F32)
+        total = mo[chip(0, core)].astype(F32)
+        for distance in (1, -1, 2, -2, 4):
+            total = total + mo[chip(distance, core)].astype(F32)
         halves.append(total)
     pieces = []
     for j in range(ny):
@@ -420,7 +478,7 @@
             rcopy(xs.at[0, j], xs.at[1, j], ag_send.at[0, 0], ag_recv.at[0, 1, j], r_dev).start()
             rcopy(xs.at[0, j], xs.at[5, j], ag_send.at[1, 0], ag_recv.at[1, 1, j], l_dev).start()
 
-    for load in loads[1:]:
+    for load in loads:
         load.wait()
     for swap in swaps:
         swap.wait()
@@ -429,34 +487,31 @@
     top = pl.ds(0, nsp)
     low = pl.ds(nsp, nsp)
 
-    def add_chunk(x, j, first):
-        n = x.shape[0]
+    def add_chunk(rows, j):
+        n = rows.shape[0]
         w = wgu[pl.ds(pl.multiple_of(j * width, width), width), :]
-        g = dot(x, w)
-
-        @pl.when(first)
-        def _():
-            acc[0:n] = g
-
-        @pl.when(jnp.logical_not(first))
-        def _():
-            acc[0:n] += g
-
-    def finish(n, store):
-        g = acc[0:n, 0 : 2 * ff]
-        u = acc[0:n, 2 * ff : 4 * ff]
-        hidden = (silu(g) * u).astype(BF16)
-        for j in range(NCH):
-            store(j, dot(hidden, wdn[:, j * width : (j + 1) * width]))
-
-    def store_own(j, z):
-        zs[0, j] = z
+        acc[0:n] = jnp.where(j == 0, 0.0, acc[0:n]) + dot(rows, w)
+
+    def activate(n):
+        hidden[0:n] = (silu(acc[0:n, 0 : 2 * ff]) * acc[0:n, 2 * ff : 4 * ff]).astype(BF16)
+
+    def down(n, j):
+        return dot(hidden[0:n], wdn[:, pl.ds(pl.multiple_of(j * width, width), width)])
+
+    def down_pair(k, j):
+        z = down(2 * rows1, j)
+        zs[k, j] = z[0:rows1]
+        zs[4 + k, j] = z[rows1 : 2 * rows1]
 
     @pl.loop(0, NCH)
     def _(j):
-        add_chunk(xs[0, j], j, j == 0)
-
-    finish(rows1, store_own)
+        add_chunk(xs[0, j], j)
+
+    activate(rows1)
+
+    @pl.loop(0, NCH)
+    def _(j):
+        zs[0, j] = down(rows1, j)
 
     @pl.loop(0, 3 * NCH)
     def _(t):
@@ -479,23 +534,36 @@
                 xs.at[7, j, low], xs.at[4, j, low], ag_send.at[1, 3], ag_recv.at[1, 4, j], l_dev
             ).start()
 
-        add_chunk(jnp.concatenate([xs[k, j], xs[4 + k, j]], axis=0), j, j == 0)
+        add_chunk(jnp.concatenate([xs[k, j], xs[4 + k, j]], axis=0), j)
+
+        @pl.when(k > 1)
+        def _():
+            down_pair(k - 1, j)
 
         @pl.when(j == NCH - 1)
         def _():
-            def store(i, z):
-                zs[k, i] = z[0:rows1]
-                zs[4 + k, i] = z[rows1 : 2 * rows1]
-
-            finish(2 * rows1, store)
+            activate(2 * rows1)
 
     @pl.loop(0, NCH)
     def _(j):
+        down_pair(3, j)
+        sp_b[2, j, nsp:rows1] = zs[7, j, nsp:rows1].astype(BF16)
+        sn_b[2, j, 0:nsp] = zs[3, j, 0:nsp].astype(BF16)
+        rcopy(
+            sp_b.at[2, j, low], rp_b.at[2, j, low], rs_send.at[0, 2], rs_recv.at[0, 2, j], r_dev
+        ).start()
+        rcopy(
+            sn_b.at[2, j, top], rn_b.at[2, j, top], rs_send.at[1, 2], rs_recv.at[1, 2, j], l_dev
+        ).start()
         wait_bytes(xs.at[4, j, top], ag_recv.at[0, 4, j])
         wait_bytes(xs.at[4, j, low], ag_recv.at[1, 4, j])
-        add_chunk(xs[4, j], j, j == 0)
-
-    def store_far(j, z):
+        add_chunk(xs[4, j], j)
+
+    activate(rows1)
+
+    @pl.loop(0, NCH)
+    def _(j):
+        z = down(rows1, j)
         sp_b[3, j, 0:nsp] = z[0:nsp].astype(BF16)
         sn_b[3, j, nsp:rows1] = z[nsp:rows1].astype(BF16)
         rcopy(
@@ -505,31 +573,27 @@
             sn_b.at[3, j, low], rn_b.at[3, j, low], rs_send.at[1, 3], rs_recv.at[1, 3, j], l_dev
         ).start()
 
-    finish(rows1, store_far)
-
-    @pl.loop(0, 3 * NCH)
+    @pl.loop(0, NCH)
+    def _(j):
+        wait_bytes(rp_b.at[3, j, top], rs_recv.at[0, 3, j])
+        wait_bytes(rn_b.at[3, j, low], rs_recv.at[1, 3, j])
+        sp_b[2, j, 0:nsp] = (zs[7, j, 0:nsp] + rp_b[3, j, 0:nsp].astype(F32)).astype(BF16)
+        sn_b[2, j, nsp:rows1] = (zs[3, j, nsp:rows1] + rn_b[3, j, nsp:rows1].astype(F32)).astype(BF16)
+        rcopy(
+            sp_b.at[2, j, top], rp_b.at[2, j, top], rs_send.at[0, 2], rs_recv.at[0, 2, j], r_dev
+        ).start()
+        rcopy(
+            sn_b.at[2, j, low], rn_b.at[2, j, low], rs_send.at[1, 2], rs_recv.at[1, 2, j], l_dev
+        ).start()
+
+    @pl.loop(0, 2 * NCH)
     def _(t):
-        k = 3 - t // NCH
+        k = 2 - t // NCH
         j = t % NCH
-
-        @pl.when(k == 3)
-        def _():
-            wait_bytes(rp_b.at[3, j, top], rs_recv.at[0, 3, j])
-            wait_bytes(rn_b.at[3, j, low], rs_recv.at[1, 3, j])
-            sp_b[2, j, 0:nsp] = (zs[7, j, 0:nsp] + rp_b[3, j, 0:nsp].astype(F32)).astype(BF16)
-            sp_b[2, j, nsp:rows1] = zs[7, j, nsp:rows1].astype(BF16)
-            sn_b[2, j, 0:nsp] = zs[3, j, 0:nsp].astype(BF16)
-            sn_b[2, j, nsp:rows1] = (
-                zs[3, j, nsp:rows1] + rn_b[3, j, nsp:rows1].astype(F32)
-            ).astype(BF16)
-
-        @pl.when(k < 3)
-        def _():
-            wait_bytes(rp_b.at[k, j], rs_recv.at[0, k, j])
-            wait_bytes(rn_b.at[k, j], rs_recv.at[1, k, j])
-            sp_b[k - 1, j] = (zs[4 + k, j] + rp_b[k, j].astype(F32)).astype(BF16)
-            sn_b[k - 1, j] = (zs[k, j] + rn_b[k, j].astype(F32)).astype(BF16)
-
+        wait_bytes(rp_b.at[k, j], rs_recv.at[0, k, j])
+        wait_bytes(rn_b.at[k, j], rs_recv.at[1, k, j])
+        sp_b[k - 1, j] = (zs[4 + k, j] + rp_b[k, j].astype(F32)).astype(BF16)
+        sn_b[k - 1, j] = (zs[k, j] + rn_b[k, j].astype(F32)).astype(BF16)
         rcopy(
             sp_b.at[k - 1, j], rp_b.at[k - 1, j], rs_send.at[0, k - 1], rs_recv.at[0, k - 1, j], r_dev
         ).start()
@@ -571,8 +635,17 @@
     wait_bytes(tot_r.at[pl.ds(0, others)], tsem.at[0])
     wait_bytes(st_r.at[pl.ds(0, others)], ssem.at[0])
     wait_bytes(sc_r.at[pl.ds(0, others)], osem.at[0])
-    wait_bytes(wc.at[:, pl.ds(0, 128 * (ny - 1))], wsem.at[0])
-    wait_bytes(mo.at[pl.ds(0, ntp - 1)], psem.at[0])
+    wait_bytes(far_w, wsem.at[0])
+
+    @pl.when(x > 0)
+    def _():
+        wait_bytes(w_block(0), wsend.at[0])
+
+    for m in range(1, turns):
+        wait_bytes(w_block(0), wsend.at[m])
+    wait_bytes(mo.at[pl.ds(0, ntp - 5)], psem.at[0])
+    for copy in relays:
+        copy.wait_send()
     for p in range(parts):
         wait_bytes(dr.at[p, pl.ds(0, others)], dsem.at[0, p])
         wait_bytes(br.at[p, pl.ds(0, others)], bsem.at[0, p])
@@ -621,8 +694,9 @@
         pltpu.VMEM((16, 512), BF16),
         pltpu.VMEM((16, 512), BF16),
         pltpu.VMEM((tokens + 32, 512), F32),
-        pltpu.VMEM((8, 128), F32),
-        pltpu.VMEM((nsp, 8, 128), F32),
+        pltpu.VMEM((1, 128), F32),
+        pltpu.VMEM((nsp, 1, 128), F32),
+        pltpu.VMEM((2, nsp, 128), F32),
         pltpu.VMEM(pair, BF16),
         pltpu.VMEM(pair, BF16),
         pltpu.VMEM(pair, F32),
@@ -632,6 +706,8 @@
         pltpu.VMEM((chan, 128 * ny), BF16),
         pltpu.VMEM((ntp, own, 128 * ny), BF16),
         pltpu.VMEM((ntp, own, 128 * ny), BF16),
+        pltpu.VMEM((2, 2, own, 128 * ny), BF16),
+        pltpu.VMEM((2, 2, own, 128 * ny), BF16),
         pltpu.VMEM(msg, BF16),
         pltpu.VMEM(msg, BF16),
         pltpu.VMEM((nsp * WIDE // 64, 128), F32),
@@ -639,6 +715,7 @@
         pltpu.VMEM((wg.shape[1], 4 * ff), BF16),
         pltpu.VMEM((2 * ff, wd.shape[2]), BF16),
         pltpu.VMEM((2 * rows1, 4 * ff), F32),
+        pltpu.VMEM((2 * rows1, 2 * ff), BF16),
         pltpu.VMEM((8, NCH, rows1, width), F32),
         pltpu.VMEM(ring, BF16),
         pltpu.VMEM(ring, BF16),
@@ -646,15 +723,18 @@
         pltpu.VMEM(ring, BF16),
         pltpu.VMEM(msg, BF16),
         pltpu.VMEM(msg, BF16),
-        dma((4,)),
+        dma((3,)),
         dma((4,)),
         dma((2,)),
         dma((2,)),
         dma((2,)),
         dma((2,)),
         dma((2,)),
+        dma((ny // NX,)),
+        dma((ny // NX,)),
         dma((6,)),
         dma((2,)),
+        dma((2, 2, 2)),
         dma((2, parts)),
         dma((2, 4)),
         dma((2, 5, NCH)),

time: 118 us -> 111 us (0.941)
  Pallas kernels: 115 us -> 109 us
    pallas_call x1, Pallas kernels: 115 us -> 109 us  [layer(): pl.pallas_call(functools.partial(body, nsp, ntp), out_shape=jax.ShapeDtyp...]
where the time goes in v3:
time: 111 us
  Pallas kernels  109 us (98%)
  local copies, waits for them, and re-layouts  1.47 us (1%)
    pallas_call x1, Pallas kernels, layer(): pl.pallas_call(functools.partial(body, nsp, ntp), out_shape=jax.ShapeDtyp...  109 us

profile of v3, /device:TPU:6, one launch (start us, length us, event | category | flops | bytes accessed | tf_op | source)
XLA Modules:
  0.0 110.5 jit_solution(1406069391394873137)
XLA Ops:
  0.0 109.1 %layer.1 = bf16[16,2048]{1,0:T(8,128)(2,1)} custom-call(bf16[16,2048]{1,0:T(8,128)(2,1)} %refs_0_.1, bf16[256,256]{1,0:T(8,128)(2,1)} %refs_1_.1, bf16[256,128]{1,0:T(8,128)(2,1)} %refs_2_.1, bf16[256,128]{1,0:T(8,128)(2,1)} %refs_3_.1, bf16[256,256]{1,0:T(8,128)(2,1)} %refs_4_.1, bf16[2,4,256]{2,1,0:T(4,128)(2,1)} %bitcast.13, f32[2,4]{1,0:T(2,128)} %refs_6_.1, ...), custom_call_target="tpu_custom_call" | custom-call | tf_op jit(solution)/shard_map/layer/pallas_call | solution.py:746
  109.1 1.5 %copy.21 = bf16[16,2048]{1,0:T(8,128)(2,1)} copy(bf16[16,2048]{1,0:T(8,128)(2,1)} %layer.1) | data formatting | bytes 131072

commit v4 on v3

--- a/solution.py
+++ b/solution.py
@@ -98,8 +98,8 @@
     osem,
     hdsem,
     wsem,
-    wsend,
-    wrecv,
+    wnear,
+    wfar,
     swsem,
     psem,
     nsem,
@@ -140,7 +140,6 @@
     chan = wout.shape[0] // ny
     nx = NX
     x = me % nx
-    turns = ny // nx
 
     def w_rows(of):
         return wout.at[pl.ds(pl.multiple_of(of * chan, chan), chan)]
@@ -148,17 +147,47 @@
     def w_block(of):
         return wc.at[:, pl.ds(pl.multiple_of(of * 128, 128), 128)]
 
-    @pl.when(x == 0)
-    def _():
-        pltpu.make_async_copy(w_rows(y), w_block(y), wrecv.at[0]).start()
-
     loads = [
+        pltpu.make_async_copy(w_rows(y), w_block(y), lsem.at[3]),
         pltpu.make_async_copy(wg, wgu.at[:, pl.ds(0, ff)], lsem.at[0]),
         pltpu.make_async_copy(wu, wgu.at[:, pl.ds(2 * ff, ff)], lsem.at[1]),
         pltpu.make_async_copy(wd, wdn.at[pl.ds(0, ff)], lsem.at[2]),
     ]
     for load in loads:
         load.start()
+
+    tokens = v_in.shape[0]
+    for n in (1, 2, 3):
+        inputs[n].wait()
+
+    pl.semaphore_wait(bar, nsp - 1 + ntp - 1)
+
+    right = {"sp": (me + 1) % nsp}
+    left = {"sp": (me + nsp - 1) % nsp}
+    for ref, lo, width in ((v_in, 0, 256), (k_in, 256, 128), (q_in, 384, 128)):
+        cols = pl.ds(lo, width)
+        rcopy(ref.at[pl.ds(tokens - 16, 16)], hl.at[:, cols], hsem.at[0], hsem.at[1], right).start()
+        rcopy(ref.at[pl.ds(0, 16)], hr.at[:, cols], hsem.at[2], hsem.at[3], left).start()
+
+    far = 2 + x
+
+    def w_send(distance, send, recv):
+        dst = (y + ny - distance) % ny
+        return rcopy(w_rows(dst), w_block(y), send, recv, {"tp": dst * 2 + c})
+
+    @pl.when(x > 0)
+    def _():
+        w_send(far, wfar.at[0], wfar.at[1]).start()
+
+    for distance in (1, -1, 2, -2):
+        w_send(distance, wnear.at[0], wnear.at[1]).start()
+
+    def w_relay():
+        block = w_block((y + far) % ny)
+        wait_bytes(block, wfar.at[1])
+        for i in range(1, nx):
+            to = me - x + (x + i) % nx
+            rcopy(block, block, wsem.at[0], wsem.at[1], {"sp": to}).start()
 
     for n in (5, 6, 7):
         inputs[n].wait()
@@ -203,46 +232,15 @@
         e = jnp.exp(tot_c[b][first : first + 4])
         return jnp.concatenate([jnp.broadcast_to(e[h : h + 1], (64, 128)) for h in range(4)], axis=0)
 
-    tokens = v_in.shape[0]
-    for n in (1, 2, 3):
-        inputs[n].wait()
+    @pl.loop(0, nsp - 1)
+    def _(i):
+        rcopy(tot_s, tot_r.at[me], tsem.at[0], tsem.at[1], {"sp": peer(i, me, nsp)}).start()
+
     pad[16 : 16 + tokens, 0:256] = v_in[...].astype(F32)
     pad[16 : 16 + tokens, 256:384] = k_in[...].astype(F32)
     pad[16 : 16 + tokens, 384:512] = q_in[...].astype(F32)
     for n in (0, 4, *range(8, NSMALL)):
         inputs[n].wait()
-
-    pl.semaphore_wait(bar, nsp - 1 + ntp - 1)
-
-    right = {"sp": (me + 1) % nsp}
-    left = {"sp": (me + nsp - 1) % nsp}
-    for ref, lo, width in ((v_in, 0, 256), (k_in, 256, 128), (q_in, 384, 128)):
-        cols = pl.ds(lo, width)
-        rcopy(ref.at[pl.ds(tokens - 16, 16)], hl.at[:, cols], hsem.at[0], hsem.at[1], right).start()
-        rcopy(ref.at[pl.ds(0, 16)], hr.at[:, cols], hsem.at[2], hsem.at[3], left).start()
-
-    @pl.loop(0, nsp - 1)
-    def _(i):
-        rcopy(tot_s, tot_r.at[me], tsem.at[0], tsem.at[1], {"sp": peer(i, me, nsp)}).start()
-
-    def w_send(m):
-        dst = (y + ny - x - m * nx) % ny
-        return rcopy(w_rows(dst), w_block(y), wsend.at[m], wrecv.at[m], {"tp": dst * 2 + c})
-
-    @pl.when(x > 0)
-    def _():
-        w_send(0).start()
-
-    for m in range(1, turns):
-        w_send(m).start()
-
-    def w_relay(m):
-        block = w_block((y + x + m * nx) % ny)
-        wait_bytes(block, wrecv.at[m])
-        for i in range(1, nx):
-            to = me - x + (x + i) % nx
-            rcopy(block, block, wsem.at[0], wsem.at[1], {"sp": to}).start()
-
     wait_bytes(hl, hsem.at[1])
     wait_bytes(hr, hsem.at[3])
     pad[0:16] = jnp.where(me > 0, hl[...].astype(F32), 0.0)
@@ -327,28 +325,29 @@
     mix_hi = mixing.astype(BF16)
     mix_lo = (mixing - mix_hi.astype(F32)).astype(BF16)
 
-    w_relay(0)
+    @pl.when(x > 0)
+    def _():
+        w_relay()
 
     wait_bytes(tot_r.at[pl.ds(0, others)], tsem.at[1])
-    wait_bytes(st_r.at[pl.ds(0, others)], ssem.at[1])
     head = me // (64 // piece)
     totals = jnp.concatenate([tot_r[d] for d in range(nsp)], axis=0)
     for n in range(2):
         of_head = jnp.sum(jnp.where(lane == head + 4 * n, totals, 0.0), axis=1, keepdims=True)
         decay[n] = jnp.broadcast_to(of_head, (nsp, 128))
 
-    def forward(d, carry):
-        sc_f[d, 0:piece] = carry
-        return decay[0, pl.ds(d, 1), :] * carry + st_r[d].astype(F32)[0:piece]
-
-    def backward(i, carry):
+    def scan(i, carry):
         d = nsp - 1 - i
-        sc_f[d, piece : 2 * piece] = carry
-        return decay[1, pl.ds(d, 1), :] * carry + st_r[d].astype(F32)[piece : 2 * piece]
-
+        sc_f[i, 0:piece] = carry[0]
+        sc_f[d, piece : 2 * piece] = carry[1]
+        return (
+            decay[0, pl.ds(i, 1), :] * carry[0] + st_r[i].astype(F32)[0:piece],
+            decay[1, pl.ds(d, 1), :] * carry[1] + st_r[d].astype(F32)[piece : 2 * piece],
+        )
+
+    wait_bytes(st_r.at[pl.ds(0, others)], ssem.at[1])
     zero = jnp.zeros((piece, 128), F32)
-    lax.fori_loop(0, nsp, forward, zero)
-    lax.fori_loop(0, nsp, backward, zero)
+    lax.fori_loop(0, nsp, scan, (zero, zero), unroll=8)
     sc_s[...] = sc_f[...].astype(BF16)
 
     @pl.loop(0, nsp - 1)
@@ -357,9 +356,6 @@
         rcopy(sc_s.at[dst], sc_r.at[me], osem.at[0], osem.at[1], {"sp": dst}).start()
 
     sc_r[me] = sc_s[me]
-    for m in range(1, turns):
-        w_relay(m)
-
     wait_bytes(sc_r.at[pl.ds(0, others)], osem.at[1])
 
     around = sc_r[...].astype(F32)
@@ -367,24 +363,41 @@
     leave = around[:, piece : 2 * piece].reshape(256, 128)
     enters = [enter, head_rows(0, 0) * enter + part[0][0:256]]
     leaves = [head_rows(1, 4) * leave + part[1][256:512], leave]
-    group = (iota((256, 256), 0) // 64 == iota((256, 256), 1) // 64).astype(F32) * (1.0 / 64.0)
+    group = jnp.where(iota((256, 256), 0) // 64 == iota((256, 256), 1) // 64, 1.0 / 64.0, 0.0).astype(BF16)
+    swap_h = []
     for b in range(2):
         rows = slice(b * BLOCK, (b + 1) * BLOCK)
         state = jnp.concatenate([enters[b], leaves[b]], axis=0).astype(BF16)
         read = dot(queries[rows], state, ((1,), (1,))) * rd_x[b]
         gated = (inner[b] + read[:, 0:256] + read[:, 256:512]) * gate_act[rows]
-        mean = dot(gated * gated, group, precision=HIGH)
+        square = gated * gated
+        square_hi = square.astype(BF16)
+        mean = dot(square_hi, group) + dot((square - square_hi.astype(F32)).astype(BF16), group)
         normed = gated * lax.rsqrt(mean + EPS) * gain_in[...]
         heads[c, rows, :] = normed.astype(BF16)
-
-    swap_h = rcopy(heads.at[c], heads.at[c], hdsem.at[0], hdsem.at[1], {"tp": partner})
-    swap_h.start()
-
-    far_w = wc.at[:, pl.ds(0, 128 * (ny - turns))]
-    wait_bytes(far_w, wsem.at[1])
+        half = heads.at[c, pl.ds(b * BLOCK, BLOCK)]
+        copy = rcopy(half, half, hdsem.at[0, b], hdsem.at[1, b], {"tp": partner})
+        copy.start()
+        swap_h.append(copy)
+
+    def blocks(n):
+        return wc.at[:, pl.ds(0, 128 * n)]
+
+    loads[0].wait()
+    wait_bytes(blocks(4), wnear.at[1])
+
+    @pl.when(x == 0)
+    def _():
+        wait_bytes(blocks(nx - 1), wsem.at[1])
+
+    @pl.when(x > 0)
+    def _():
+        wait_bytes(blocks(nx - 2), wsem.at[1])
+
     inner_c = chan // 2
     own_part = dot(heads[c], wc[pl.ds(pl.multiple_of(c * inner_c, inner_c), inner_c), :])
-    swap_h.wait()
+    for copy in swap_h:
+        copy.wait()
     o_c = 1 - c
     full = own_part + dot(heads[o_c], wc[pl.ds(pl.multiple_of(o_c * inner_c, inner_c), inner_c), :])
     po[...] = full.reshape(ntp, own, full.shape[1]).astype(BF16)
@@ -478,7 +491,7 @@
             rcopy(xs.at[0, j], xs.at[1, j], ag_send.at[0, 0], ag_recv.at[0, 1, j], r_dev).start()
             rcopy(xs.at[0, j], xs.at[5, j], ag_send.at[1, 0], ag_recv.at[1, 1, j], l_dev).start()
 
-    for load in loads:
+    for load in loads[1:]:
         load.wait()
     for swap in swaps:
         swap.wait()
@@ -635,14 +648,13 @@
     wait_bytes(tot_r.at[pl.ds(0, others)], tsem.at[0])
     wait_bytes(st_r.at[pl.ds(0, others)], ssem.at[0])
     wait_bytes(sc_r.at[pl.ds(0, others)], osem.at[0])
-    wait_bytes(far_w, wsem.at[0])
+    wait_bytes(blocks(4), wnear.at[0])
 
     @pl.when(x > 0)
     def _():
-        wait_bytes(w_block(0), wsend.at[0])
-
-    for m in range(1, turns):
-        wait_bytes(w_block(0), wsend.at[m])
+        wait_bytes(blocks(1), wfar.at[0])
+        wait_bytes(blocks(nx - 1), wsem.at[0])
+
     wait_bytes(mo.at[pl.ds(0, ntp - 5)], psem.at[0])
     for copy in relays:
         copy.wait_send()
@@ -723,15 +735,15 @@
         pltpu.VMEM(ring, BF16),
         pltpu.VMEM(msg, BF16),
         pltpu.VMEM(msg, BF16),
-        dma((3,)),
+        dma((4,)),
         dma((4,)),
         dma((2,)),
         dma((2,)),
         dma((2,)),
+        dma((2, 2)),
         dma((2,)),
         dma((2,)),
-        dma((ny // NX,)),
-        dma((ny // NX,)),
+        dma((2,)),
         dma((6,)),
         dma((2,)),
         dma((2, 2, 2)),

time: 111 us -> 108 us (0.973)
  Pallas kernels: 109 us -> 106 us
    pallas_call x1, Pallas kernels: 109 us -> 106 us  [layer(): pl.pallas_call(functools.partial(body, nsp, ntp), out_shape=jax.ShapeDtyp...]
where the time goes in v4:
time: 108 us
  Pallas kernels  106 us (98%)
  local copies, waits for them, and re-layouts  1.47 us (1%)
    pallas_call x1, Pallas kernels, layer(): pl.pallas_call(functools.partial(body, nsp, ntp), out_shape=jax.ShapeDtyp...  106 us

profile of v4, /device:TPU:6, one launch (start us, length us, event | category | flops | bytes accessed | tf_op | source)
XLA Modules:
  0.0 107.7 jit_solution(14974334945858607562)
XLA Ops:
  0.0 106.2 %layer.1 = bf16[16,2048]{1,0:T(8,128)(2,1)} custom-call(bf16[16,2048]{1,0:T(8,128)(2,1)} %refs_0_.1, bf16[256,256]{1,0:T(8,128)(2,1)} %refs_1_.1, bf16[256,128]{1,0:T(8,128)(2,1)} %refs_2_.1, bf16[256,128]{1,0:T(8,128)(2,1)} %refs_3_.1, bf16[256,256]{1,0:T(8,128)(2,1)} %refs_4_.1, bf16[2,4,256]{2,1,0:T(4,128)(2,1)} %bitcast.13, f32[2,4]{1,0:T(2,128)} %refs_6_.1, ...), custom_call_target="tpu_custom_call" | custom-call | tf_op jit(solution)/shard_map/layer/pallas_call | solution.py:758
  106.2 1.5 %copy.21 = bf16[16,2048]{1,0:T(8,128)(2,1)} copy(bf16[16,2048]{1,0:T(8,128)(2,1)} %layer.1) | data formatting | bytes 131072

commit v5 on v4

--- a/solution.py
+++ b/solution.py
@@ -76,6 +76,10 @@
     mo,
     near,
     through,
+    sm,
+    sr,
+    xsc,
+    acc_own,
     dm,
     dr,
     rowsf,
@@ -103,6 +107,9 @@
     swsem,
     psem,
     nsem,
+    csem,
+    xsend,
+    xrecv,
     dsem,
     ag_send,
     ag_recv,
@@ -315,8 +322,10 @@
     w_lane = iota((tiles * own, own), 0) % own == iota((tiles * own, own), 1)
     mixing = jnp.zeros(r_id.shape, F32)
     place = jnp.zeros(r_id.shape, F32)
+    slots = []
     for n in range(2):
         slot = jnp.sum(hots[n] * ids, axis=1, keepdims=True)
+        slots.append(slot)
         hit = same & (r_slot == jnp.concatenate([slot] * tiles, axis=0))
         weight = jnp.sum(jnp.where(w_lane, cw_in[n : n + 1], 0.0), axis=1, keepdims=True)
         place = jnp.where(hit, 1.0, place)
@@ -400,36 +409,55 @@
         copy.wait()
     o_c = 1 - c
     full = own_part + dot(heads[o_c], wc[pl.ds(pl.multiple_of(o_c * inner_c, inner_c), inner_c), :])
-    po[...] = full.reshape(ntp, own, full.shape[1]).astype(BF16)
+    span = full.shape[1] // 2
+    for h in range(2):
+        po[h] = full[:, h * span : (h + 1) * span].reshape(ntp, own, span).astype(BF16)
 
     def chip(distance, core):
         return ((y + ny + distance) % ny) * 2 + core
 
-    relays = []
-    for way in range(2):
-        sign = 1 - 2 * way
-        for core in range(2):
-            copy = rcopy(
-                po.at[chip(3 * sign, core)],
-                near.at[way, core],
-                nsem.at[0, way, core],
-                nsem.at[1, way, core],
-                {"tp": chip(sign, c)},
-            )
-            copy.start()
-            relays.append(copy)
-    for distance in (4, 1, -1):
-        for core in range(2):
-            dst = chip(distance, core)
-            rcopy(po.at[dst], mo.at[tp], psem.at[0], psem.at[1], {"tp": dst}).start()
-    rcopy(po.at[partner], mo.at[tp], psem.at[0], psem.at[1], {"tp": partner}).start()
-    mo[tp] = po[tp]
-    for way in range(2):
-        for core in range(2):
-            dst = chip(2 - 4 * way, core)
-            relays[2 * way + core].wait_recv()
-            through[way, core] = (po[dst].astype(F32) + near[way, core].astype(F32)).astype(BF16)
-            rcopy(through.at[way, core], mo.at[tp], psem.at[0], psem.at[1], {"tp": dst}).start()
+    relays = [[], []]
+
+    def send_far(h):
+        for way in range(2):
+            sign = 1 - 2 * way
+            for core in range(2):
+                copy = rcopy(
+                    po.at[h, chip(3 * sign, core)],
+                    near.at[h, way, core],
+                    nsem.at[0, h, way, core],
+                    nsem.at[1, h, way, core],
+                    {"tp": chip(sign, c)},
+                )
+                copy.start()
+                relays[h].append(copy)
+
+    def send_direct(h):
+        for distance in (4, 1, -1):
+            for core in range(2):
+                dst = chip(distance, core)
+                rcopy(po.at[h, dst], mo.at[h, tp], psem.at[0, h], psem.at[1, h], {"tp": dst}).start()
+        rcopy(po.at[h, partner], mo.at[h, tp], psem.at[0, h], psem.at[1, h], {"tp": partner}).start()
+        mo[h, tp] = po[h, tp]
+
+    def send_through(h):
+        for way in range(2):
+            for core in range(2):
+                dst = chip(2 - 4 * way, core)
+                relays[h][2 * way + core].wait_recv()
+                through[h, way, core] = (
+                    po[h, dst].astype(F32) + near[h, way, core].astype(F32)
+                ).astype(BF16)
+                rcopy(
+                    through.at[h, way, core], mo.at[h, tp], psem.at[0, h], psem.at[1, h], {"tp": dst}
+                ).start()
+
+    send_far(0)
+    send_direct(0)
+    send_far(1)
+    send_through(0)
+    send_direct(1)
+    send_through(1)
 
     swaps = [
         rcopy(wg, wgu.at[:, pl.ds(ff, ff)], swsem.at[0], swsem.at[1], {"tp": partner}),
@@ -439,42 +467,65 @@
     for swap in swaps:
         swap.start()
 
-    wait_bytes(mo.at[pl.ds(0, ntp - 5)], psem.at[1])
-    halves = []
-    for core in range(2):
-        total = mo[chip(0, core)].astype(F32)
-        for distance in (1, -1, 2, -2, 4):
-            total = total + mo[chip(distance, core)].astype(F32)
-        halves.append(total)
-    pieces = []
-    for j in range(ny):
-        pieces += [halves[0][:, 128 * j : 128 * j + 128], halves[1][:, 128 * j : 128 * j + 128]]
-    mixer_out = jnp.concatenate(pieces, axis=1).astype(BF16).astype(F32)
-    middle = (resid[...].astype(F32) + mixer_out).astype(BF16).astype(F32)
-    square = jnp.mean(middle * middle, axis=-1, keepdims=True)
-    normed = (middle * lax.rsqrt(square + EPS) * ngain_in[...]).astype(BF16)
-    parts = normed.shape[1] // WIDE
-    width = normed.shape[1] // NCH
+    parts = resid.shape[1] // WIDE
+    width = resid.shape[1] // NCH
     per = NCH // parts
-    stacked = jnp.concatenate(
-        [
-            jnp.concatenate(
-                [normed[:, p * WIDE + n * 128 : p * WIDE + (n + 1) * 128] for n in range(tiles)], axis=0
-            )
-            for p in range(parts)
-        ],
-        axis=1,
-    )
-    sent = dot(place, stacked, first)
-    for p in range(parts):
-        dm[p] = sent[:, p * 128 : (p + 1) * 128].reshape(nsp, 2 * tiles, 128).astype(BF16)
-
-        @pl.loop(0, nsp - 1)
-        def _(i):
-            dst = peer(i, me, nsp)
-            rcopy(dm.at[p, dst], dr.at[p, me], dsem.at[0, p], dsem.at[1, p], {"sp": dst}).start()
-
-        dr[p, me] = dm[p, me]
+    piled = parts // 2
+    middles = []
+    squares = jnp.zeros((own, 1), F32)
+    for h in range(2):
+        wait_bytes(mo.at[h, pl.ds(0, ntp - 5)], psem.at[1, h])
+        halves = []
+        for core in range(2):
+            total = mo[h, chip(0, core)].astype(F32)
+            for distance in (1, -1, 2, -2, 4):
+                total = total + mo[h, chip(distance, core)].astype(F32)
+            halves.append(total)
+        pieces = []
+        for j in range(span // 128):
+            pieces += [halves[0][:, 128 * j : 128 * j + 128], halves[1][:, 128 * j : 128 * j + 128]]
+        mixer_out = jnp.concatenate(pieces, axis=1).astype(BF16).astype(F32)
+        cols = slice(h * 2 * span, (h + 1) * 2 * span)
+        middle = (resid[:, cols].astype(F32) + mixer_out).astype(BF16).astype(F32)
+        middles.append(middle)
+        squares = squares + jnp.sum(middle * middle, axis=-1, keepdims=True)
+        rows = (middle * ngain_in[:, cols]).astype(BF16)
+        stacked = jnp.concatenate(
+            [
+                jnp.concatenate(
+                    [rows[:, q * WIDE + n * 128 : q * WIDE + (n + 1) * 128] for n in range(tiles)], axis=0
+                )
+                for q in range(piled)
+            ],
+            axis=1,
+        )
+        sent = dot(place, stacked, first)
+        for q in range(piled):
+            p = h * piled + q
+            dm[p] = sent[:, q * 128 : (q + 1) * 128].reshape(nsp, 2 * tiles, 128).astype(BF16)
+
+            @pl.loop(0, nsp - 1)
+            def _(i):
+                dst = peer(i, me, nsp)
+                rcopy(dm.at[p, dst], dr.at[p, me], dsem.at[0, p], dsem.at[1, p], {"sp": dst}).start()
+
+            dr[p, me] = dm[p, me]
+
+    inverse = lax.rsqrt(squares * (1.0 / resid.shape[1]) + EPS)
+    scales = jnp.zeros((nsp, 128), F32)
+    for n in range(2):
+        wanted = (iota((own, nsp), 1) * 2 + n).astype(F32)
+        named = ((slots[0] == wanted) | (slots[1] == wanted)).astype(F32)
+        scales = scales + dot(named, jnp.where(lane == n, inverse, 0.0), first, HIGH)
+    for e in range(nsp):
+        sm[e] = scales[e : e + 1]
+
+    @pl.loop(0, nsp - 1)
+    def _(i):
+        dst = peer(i, me, nsp)
+        rcopy(sm.at[dst], sr.at[me], csem.at[0], csem.at[1], {"sp": dst}).start()
+
+    sr[me] = sm[me]
 
     r_dev = {"tp": right_y}
     l_dev = {"tp": left_y}
@@ -500,13 +551,24 @@
     top = pl.ds(0, nsp)
     low = pl.ds(nsp, nsp)
 
-    def add_chunk(rows, j):
+    def add_chunk(rows, j, acc):
         n = rows.shape[0]
         w = wgu[pl.ds(pl.multiple_of(j * width, width), width), :]
         acc[0:n] = jnp.where(j == 0, 0.0, acc[0:n]) + dot(rows, w)
 
-    def activate(n):
-        hidden[0:n] = (silu(acc[0:n, 0 : 2 * ff]) * acc[0:n, 2 * ff : 4 * ff]).astype(BF16)
+    def scale_of(k):
+        hit = iota((rows1, 128), 0) == iota((rows1, 128), 1)
+        return jnp.sum(jnp.where(hit, xsc[k], 0.0), axis=1, keepdims=True)
+
+    def activate(n, acc, scale):
+        gate = acc[0:n, 0 : 2 * ff] * scale
+        hidden[0:n] = (silu(gate) * (acc[0:n, 2 * ff : 4 * ff] * scale)).astype(BF16)
+
+    def send_scale(k, way):
+        at = k if way == 0 or k == 0 else 4 + k
+        to = k + 1 if way == 0 else 5 + k
+        dev = r_dev if way == 0 else l_dev
+        rcopy(xsc.at[at], xsc.at[to], xsend.at[way, k], xrecv.at[way, k + 1], dev).start()
 
     def down(n, j):
         return dot(hidden[0:n], wdn[:, pl.ds(pl.multiple_of(j * width, width), width)])
@@ -518,13 +580,17 @@
 
     @pl.loop(0, NCH)
     def _(j):
-        add_chunk(xs[0, j], j)
-
-    activate(rows1)
-
-    @pl.loop(0, NCH)
-    def _(j):
-        zs[0, j] = down(rows1, j)
+        add_chunk(xs[0, j], j, acc_own)
+
+    wait_bytes(sr.at[pl.ds(0, others)], csem.at[1])
+    given = jnp.concatenate([sr[d] for d in range(nsp)], axis=0)
+    ring_row = jnp.zeros((1, 128), F32)
+    for n in range(2):
+        spot = iota((nsp, 128), 1) == iota((nsp, 128), 0) + n * nsp
+        ring_row = ring_row + jnp.sum(jnp.where(spot, given[:, n : n + 1], 0.0), axis=0, keepdims=True)
+    xsc[0] = ring_row
+    send_scale(0, 0)
+    send_scale(0, 1)
 
     @pl.loop(0, 3 * NCH)
     def _(t):
@@ -547,7 +613,7 @@
                 xs.at[7, j, low], xs.at[4, j, low], ag_send.at[1, 3], ag_recv.at[1, 4, j], l_dev
             ).start()
 
-        add_chunk(jnp.concatenate([xs[k, j], xs[4 + k, j]], axis=0), j)
+        add_chunk(jnp.concatenate([xs[k, j], xs[4 + k, j]], axis=0), j, acc)
 
         @pl.when(k > 1)
         def _():
@@ -555,7 +621,17 @@
 
         @pl.when(j == NCH - 1)
         def _():
-            activate(2 * rows1)
+            wait_bytes(xsc.at[k], xrecv.at[0, k])
+            wait_bytes(xsc.at[4 + k], xrecv.at[1, k])
+            send_scale(k, 0)
+
+            @pl.when(k < 3)
+            def _():
+                rcopy(
+                    xsc.at[4 + k], xsc.at[5 + k], xsend.at[1, k], xrecv.at[1, k + 1], l_dev
+                ).start()
+
+            activate(2 * rows1, acc, jnp.concatenate([scale_of(k), scale_of(4 + k)], axis=0))
 
     @pl.loop(0, NCH)
     def _(j):
@@ -570,9 +646,10 @@
         ).start()
         wait_bytes(xs.at[4, j, top], ag_recv.at[0, 4, j])
         wait_bytes(xs.at[4, j, low], ag_recv.at[1, 4, j])
-        add_chunk(xs[4, j], j)
-
-    activate(rows1)
+        add_chunk(xs[4, j], j, acc)
+
+    wait_bytes(xsc.at[4], xrecv.at[0, 4])
+    activate(rows1, acc, scale_of(4))
 
     @pl.loop(0, NCH)
     def _(j):
@@ -585,6 +662,12 @@
         rcopy(
             sn_b.at[3, j, low], rn_b.at[3, j, low], rs_send.at[1, 3], rs_recv.at[1, 3, j], l_dev
         ).start()
+
+    activate(rows1, acc_own, scale_of(0))
+
+    @pl.loop(0, NCH)
+    def _(j):
+        zs[0, j] = down(rows1, j)
 
     @pl.loop(0, NCH)
     def _(j):
@@ -641,7 +724,9 @@
         mixed = dot(mix_hi, back) + dot(mix_lo, back)
         for n in range(tiles):
             cols = slice(p * WIDE + n * 128, p * WIDE + (n + 1) * 128)
-            out[:, cols] = (middle[:, cols] + mixed[n * own : (n + 1) * own]).astype(BF16)
+            local = slice(cols.start % (2 * span), cols.start % (2 * span) + 128)
+            base = middles[cols.start // (2 * span)][:, local]
+            out[:, cols] = (base + mixed[n * own : (n + 1) * own]).astype(BF16)
 
     wait_bytes(hl, hsem.at[0])
     wait_bytes(hr, hsem.at[2])
@@ -655,9 +740,15 @@
         wait_bytes(blocks(1), wfar.at[0])
         wait_bytes(blocks(nx - 1), wsem.at[0])
 
-    wait_bytes(mo.at[pl.ds(0, ntp - 5)], psem.at[0])
-    for copy in relays:
-        copy.wait_send()
+    for h in range(2):
+        wait_bytes(mo.at[h, pl.ds(0, ntp - 5)], psem.at[0, h])
+        for copy in relays[h]:
+            copy.wait_send()
+    wait_bytes(sr.at[pl.ds(0, others)], csem.at[0])
+    for k in range(4):
+        wait_bytes(xsc.at[0], xsend.at[0, k])
+    for k in range(3):
+        wait_bytes(xsc.at[0], xsend.at[1, k])
     for p in range(parts):
         wait_bytes(dr.at[p, pl.ds(0, others)], dsem.at[0, p])
         wait_bytes(br.at[p, pl.ds(0, others)], bsem.at[0, p])
@@ -716,10 +807,14 @@
         pltpu.VMEM(pair, BF16),
         pltpu.VMEM((2, tokens, 256), BF16),
         pltpu.VMEM((chan, 128 * ny), BF16),
-        pltpu.VMEM((ntp, own, 128 * ny), BF16),
-        pltpu.VMEM((ntp, own, 128 * ny), BF16),
-        pltpu.VMEM((2, 2, own, 128 * ny), BF16),
-        pltpu.VMEM((2, 2, own, 128 * ny), BF16),
+        pltpu.VMEM((2, ntp, own, 64 * ny), BF16),
+        pltpu.VMEM((2, ntp, own, 64 * ny), BF16),
+        pltpu.VMEM((2, 2, 2, own, 64 * ny), BF16),
+        pltpu.VMEM((2, 2, 2, own, 64 * ny), BF16),
+        pltpu.VMEM((nsp, 1, 128), F32),
+        pltpu.VMEM((nsp, 1, 128), F32),
+        pltpu.VMEM((8, 1, 128), F32),
+        pltpu.VMEM((rows1, 4 * ff), F32),
         pltpu.VMEM(msg, BF16),
         pltpu.VMEM(msg, BF16),
         pltpu.VMEM((nsp * WIDE // 64, 128), F32),
@@ -745,8 +840,11 @@
         dma((2,)),
         dma((2,)),
         dma((6,)),
+        dma((2, 2)),
+        dma((2, 2, 2, 2)),
         dma((2,)),
-        dma((2, 2, 2)),
+        dma((2, 4)),
+        dma((2, 5)),
         dma((2, parts)),
         dma((2, 4)),
         dma((2, 5, NCH)),

time: 108 us -> 106 us (0.981)
  Pallas kernels: 106 us -> 104 us
    pallas_call x1, Pallas kernels: 106 us -> 104 us  [layer(): pl.pallas_call(functools.partial(body, nsp, ntp), out_shape=jax.ShapeDtyp...]
where the time goes in v5:
time: 106 us; the launch traced here: 105 us
  Pallas kernels  104 us (98%)
  local copies, waits for them, and re-layouts  1.47 us (1%)
    pallas_call x1, Pallas kernels, layer(): pl.pallas_call(functools.partial(body, nsp, ntp), out_shape=jax.ShapeDtyp...  104 us

profile of v5, /device:TPU:6, one launch (start us, length us, event | category | flops | bytes accessed | tf_op | source)
XLA Modules:
  0.0 105.1 jit_solution(9275781653972226969)
XLA Ops:
  0.0 103.7 %layer.1 = bf16[16,2048]{1,0:T(8,128)(2,1)} custom-call(bf16[16,2048]{1,0:T(8,128)(2,1)} %refs_0_.1, bf16[256,256]{1,0:T(8,128)(2,1)} %refs_1_.1, bf16[256,128]{1,0:T(8,128)(2,1)} %refs_2_.1, bf16[256,128]{1,0:T(8,128)(2,1)} %refs_3_.1, bf16[256,256]{1,0:T(8,128)(2,1)} %refs_4_.1, bf16[2,4,256]{2,1,0:T(4,128)(2,1)} %bitcast.13, f32[2,4]{1,0:T(2,128)} %refs_6_.1, ...), custom_call_target="tpu_custom_call" | custom-call | tf_op jit(solution)/shard_map/layer/pallas_call | solution.py:856
  103.7 1.5 %copy.21 = bf16[16,2048]{1,0:T(8,128)(2,1)} copy(bf16[16,2048]{1,0:T(8,128)(2,1)} %layer.1) | data formatting | bytes 131072

commit v6 on v5

--- a/solution.py
+++ b/solution.py
@@ -531,7 +531,7 @@
     l_dev = {"tp": left_y}
     for p in range(parts):
         wait_bytes(dr.at[p, pl.ds(0, others)], dsem.at[1, p])
-        rowsf[...] = dr[p].astype(F32).reshape(nsp * 2 * tiles, 128)
+        rowsf[0 : nsp * 2 * tiles] = dr[p].astype(F32).reshape(nsp * 2 * tiles, 128)
         for q in range(per):
             j = p * per + q
             for n in range(width // 128):
@@ -709,7 +709,7 @@
                     rowsf[pl.ds(2 * tile + s, nsp, stride=2 * tiles), :] = total[
                         s * nsp : (s + 1) * nsp, n * 128 : (n + 1) * 128
                     ]
-        bm[p] = rowsf[...].reshape(nsp, 2 * tiles, 128).astype(BF16)
+        bm[p] = rowsf[0 : nsp * 2 * tiles].reshape(nsp, 2 * tiles, 128).astype(BF16)
 
         @pl.loop(0, nsp - 1)
         def _(i):
@@ -817,7 +817,7 @@
         pltpu.VMEM((rows1, 4 * ff), F32),
         pltpu.VMEM(msg, BF16),
         pltpu.VMEM(msg, BF16),
-        pltpu.VMEM((nsp * WIDE // 64, 128), F32),
+        pltpu.VMEM((nsp * WIDE // 64 + 8, 128), F32),
         pltpu.VMEM((8, NCH, rows1, width), BF16),
         pltpu.VMEM((wg.shape[1], 4 * ff), BF16),
         pltpu.VMEM((2 * ff, wd.shape[2]), BF16),

time: 106 us -> 106 us (level)
  no operation moved by 1% of the time
where the time goes in v6:
time: 106 us; the launch traced here: 105 us
  Pallas kernels  104 us (98%)
  local copies, waits for them, and re-layouts  1.47 us (1%)
    pallas_call x1, Pallas kernels, layer(): pl.pallas_call(functools.partial(body, nsp, ntp), out_shape=jax.ShapeDtyp...  104 us

profile of v6, /device:TPU:6, one launch (start us, length us, event | category | flops | bytes accessed | tf_op | source)
XLA Modules:
  0.0 105.2 jit_solution(7881549951325596607)
XLA Ops:
  0.0 103.7 %layer.1 = bf16[16,2048]{1,0:T(8,128)(2,1)} custom-call(bf16[16,2048]{1,0:T(8,128)(2,1)} %refs_0_.1, bf16[256,256]{1,0:T(8,128)(2,1)} %refs_1_.1, bf16[256,128]{1,0:T(8,128)(2,1)} %refs_2_.1, bf16[256,128]{1,0:T(8,128)(2,1)} %refs_3_.1, bf16[256,256]{1,0:T(8,128)(2,1)} %refs_4_.1, bf16[2,4,256]{2,1,0:T(4,128)(2,1)} %bitcast.13, f32[2,4]{1,0:T(2,128)} %refs_6_.1, ...), custom_call_target="tpu_custom_call" | custom-call | tf_op jit(solution)/shard_map/layer/pallas_call | solution.py:856
  103.7 1.5 %copy.21 = bf16[16,2048]{1,0:T(8,128)(2,1)} copy(bf16[16,2048]{1,0:T(8,128)(2,1)} %layer.1) | data formatting | bytes 131072
